TPU v7x, 512 devices: a whole 4x8x8 slice. The times are simulated.
512 devices in a mesh: sp: 64 (over z, y), tp: 8 (over x, core).
Axes of the slice: x: 4, y: 8, z: 8, core: 2. Of those that a mesh axis runs over, the one named last changes fastest.
Arguments:
- skip_stream_entering: bfloat16 [4096, 2048], P('sp'), may hold values from -6 to 6
- reading_vectors: bfloat16 [4096, 1024], P('sp', 'tp'), may hold values from -6 to 6
- blender_lookup_labels: bfloat16 [4096, 1024], P('sp', 'tp'), may hold values from -6 to 6
- blender_payloads: bfloat16 [4096, 1024], P('sp', 'tp'), may hold values from -6 to 6
- blender_result_valve: bfloat16 [4096, 1024], P('sp', 'tp'), may hold values from -6 to 6
- fading_logits: bfloat16 [2, 4096, 1024], P(None, 'sp', 'tp'), as said below
- amend_speed_logits: bfloat16 [2, 4096, 1024], P(None, 'sp', 'tp'), as said below
- extra_log_fades: float32 [2, 16, 4096], P(None, 'tp', 'sp'), may hold values from -3 to 0
- present_reward_factors: float32 [1024], P('tp'), may hold values from -1.2 to 1.2
- attender_scaling_vector: float32 [1024], P('tp'), may hold values from 0.1 to 1.9
- blender_result_projector: bfloat16 [1024, 2048], P('tp'), may hold values from -0.1875 to 0.1875
- blender_scaling_vector: float32 [2048], replicated, may hold values from 0.1 to 1.9
- perceptron_valve_factors: bfloat16 [2048, 5632], P('sp', 'tp'), may hold values from -0.125 to 0.125
- perceptron_widen_factors: bfloat16 [2048, 5632], P('sp', 'tp'), may hold values from -0.125 to 0.125
- perceptron_shrink_factors: bfloat16 [5632, 2048], P('tp', 'sp'), may hold values from -0.078125 to 0.078125
- closing_scaling_vector: float32 [2048], replicated, may hold values from 0.1 to 1.9
Outputs:
- result: bfloat16 [4096, 2048], P(('sp', 'tp'))
Inputs may be any that keep to these rules, and one draw needn't show every extreme that they name: `fading_logits`: decay pre-activations. `amend_speed_logits`: correction-rate pre-activations.
All inputs are finite; a program needn't handle non-finite values.
Results may differ from a plain program's by a relative error of at most 0.02.
Values may be sent and summed in bfloat16 or wider, within the bound.
No kernel may reach another device: no remote copies, remote signals or barrier semaphores. Data moves between devices by JAX's collectives and lax.ppermute only.
A program may use at most 64 MiB of HBM per device.

v0:
```python
import jax
import jax.numpy as jnp
from jax import lax
from jax.sharding import Mesh
from jax.sharding import PartitionSpec as P

SP = ("sp_0", "sp_1")
SP_TP = ("sp_0", "sp_1", "tp")


RESIDUAL_SCALE = 2.0**0.25
NORM_EPS = 1e-05
GROUP_EPS = 0.00064
KEY_EPS = 1e-06


def turned_gather(arrays, axis, dims):
    turned = [jnp.moveaxis(a, dim, 0) for a, dim in zip(arrays, dims)]
    widths = [t[0].size for t in turned]
    both = jnp.concatenate([t.reshape(-1, w) for t, w in zip(turned, widths)], axis=1)
    whole = lax.all_gather(both, axis, axis=0, tiled=True)
    blocks = jnp.split(whole, [sum(widths[:k]) for k in range(1, len(widths))], axis=1)
    return tuple(
        (
            jnp.moveaxis(b.reshape(-1, *t.shape[1:]), 0, dim)
            for b, t, dim in zip(blocks, turned, dims)
        )
    )


def nothing_yet(value, identity):
    return jax.tree.map(
        lambda part, zero: jnp.zeros_like(part) + jnp.asarray(zero, part.dtype), value, identity
    )


def collected_together(value, axis):
    leaves = jax.tree.leaves(value)
    order = sorted(range(len(leaves)), key=lambda k: -leaves[k].size)
    width = (1, *leaves[order[0]].shape)[-1]
    lines = [
        jnp.pad(leaves[k].reshape(-1), (0, -leaves[k].size % width)).reshape(-1, width)
        for k in order
    ]
    both, at, found = (lax.all_gather(jnp.concatenate(lines), axis), 0, {})
    for k, line in zip(order, lines):
        share = both[:, at : at + len(line)].reshape(len(both), -1)
        found[k] = share[:, : leaves[k].size].reshape(-1, *leaves[k].shape)
        at += len(line)
    numbers = iter(range(len(leaves)))
    return jax.tree.map(lambda _: found[next(numbers)], value)


def carried_in(value, axes, combine, identity, reverse):
    before = start = nothing_yet(value, identity)
    total = value
    for axis in reversed(axes):
        length, position = (lax.axis_size(axis), lax.axis_index(axis))
        pieces = collected_together(
            jax.tree.map(lambda part, kind: part.astype(kind), total, (jnp.bfloat16, jnp.bfloat16)),
            axis,
        )
        inside, total = (start, start)
        for k in reversed(range(length)) if reverse else range(length):
            passed = k > position if reverse else k < position
            total = combine(
                total, jax.tree.map(lambda part, own: part[k].astype(own.dtype), pieces, value)
            )
            inside = jax.tree.map(lambda new, old: jnp.where(passed, new, old), total, inside)
        before = combine(inside, before)
    return before


def cut_along(value, dim, length):
    before, after = (value.shape[:dim], value.shape[dim + 1 :])
    return jnp.moveaxis(value.reshape(*before, length, -1, *after), dim, 0)


def sent_and_summed(value, axis, dim):
    length = lax.axis_size(axis)
    blocks = lax.all_to_all(cut_along(value, dim, length), axis, 0, 0, tiled=True)
    return jnp.sum(blocks.astype(jnp.float32), axis=0)


def joined_along(blocks, dim):
    dims = list(blocks.shape[1:])
    dims[dim] *= blocks.shape[0]
    return jnp.moveaxis(blocks, 0, dim).reshape(dims)


def sent_to_all(value, axis):
    copies = jnp.broadcast_to(value, (lax.axis_size(axis), *value.shape))
    return lax.all_to_all(copies, axis, split_axis=0, concat_axis=0, tiled=True)


def gathered_copies(value, axis, dim):
    return joined_along(sent_to_all(value, axis), dim)


def layer_norm(summand, gain_vec):
    center = jnp.mean(summand, -1, keepdims=True)
    spread = jnp.mean(jnp.square(summand - center), -1, keepdims=True)
    return (summand - center) * lax.rsqrt(spread + NORM_EPS) * gain_vec


def chain_blocks(earlier, later):
    return (
        jnp.einsum("hij,hjk->hik", earlier[0], later[0]),
        jnp.einsum("hij,hjk->hik", earlier[1], later[0]) + later[1],
    )


def advance(joined, inputs):
    query_vec, decay_vec, write_key, padded_value, erase_vec, refill_vec = inputs
    erased = jnp.einsum("hji,hj->hi", joined, erase_vec)
    joined = (
        joined * decay_vec[:, :, None]
        + refill_vec[:, :, None] * erased[:, None, :]
        + write_key[:, :, None] * padded_value[:, None, :]
    )
    return (joined, jnp.einsum("hji,hj->hi", joined, query_vec))


def shards(
    skip_stream_entering,
    reading_vectors,
    blender_lookup_labels,
    blender_payloads,
    blender_result_valve,
    fading_logits,
    amend_speed_logits,
    extra_log_fades,
    present_reward_factors,
    attender_scaling_vector,
    blender_result_projector,
    blender_scaling_vector,
    perceptron_valve_factors,
    perceptron_widen_factors,
    perceptron_shrink_factors,
    closing_scaling_vector,
):
    whole_gate, whole_up, whole_down = turned_gather(
        (perceptron_valve_factors, perceptron_widen_factors, perceptron_shrink_factors),
        SP,
        (0, 0, 1),
    )
    tok_rows = reading_vectors.shape[0]
    local_attender_number = extra_log_fades.shape[1]
    head_size = reading_vectors.shape[1] // local_attender_number
    row_share = tok_rows // lax.axis_size("tp")
    row_start = lax.axis_index("tp") * row_share

    def split_attenders(tensor):
        return tensor.reshape(tensor.shape[:-1] + (local_attender_number, head_size))

    def both_ways(forward_part, backward_part):
        return jnp.concatenate([forward_part, jnp.flip(backward_part, 0)], axis=1)

    entire_asking_lines = split_attenders(reading_vectors.astype(jnp.float32))
    key_rows = split_attenders(blender_lookup_labels.astype(jnp.float32))
    payload_line_slab = split_attenders(blender_payloads.astype(jnp.float32))
    key_square = jnp.sum(key_rows * key_rows, -1, keepdims=True)
    unit_keys = key_rows * lax.rsqrt(key_square + KEY_EPS)
    fading_log_amount = (
        split_attenders(-jnp.exp(-jax.nn.softplus(-fading_logits.astype(jnp.float32)) - 0.5))
        + jnp.swapaxes(extra_log_fades, 1, 2)[..., None]
    )
    decays = jnp.exp(fading_log_amount)
    icl_rates = split_attenders(jax.nn.sigmoid(amend_speed_logits.astype(jnp.float32)))
    stored_label_lines = key_rows[None] * icl_rates
    refills = unit_keys[None] * icl_rates
    padded_payload = jnp.concatenate(
        [payload_line_slab, jnp.zeros_like(payload_line_slab)], axis=-1
    )
    sequence_in = (
        both_ways(entire_asking_lines, entire_asking_lines),
        both_ways(decays[0], decays[1]),
        both_ways(stored_label_lines[0], stored_label_lines[1]),
        both_ways(padded_payload, padded_payload),
        both_ways(-unit_keys, -unit_keys),
        both_ways(refills[0], refills[1]),
    )
    identity = jnp.broadcast_to(
        jnp.eye(head_size, dtype=jnp.float32), (2 * local_attender_number, head_size, head_size)
    )
    start_joined = jnp.concatenate([jnp.zeros_like(identity), identity], axis=-1)
    joined_end, readings = lax.scan(advance, start_joined, sequence_in, unroll=16)
    state_end = jnp.swapaxes(joined_end[..., :head_size], 1, 2)
    prod_end = jnp.swapaxes(joined_end[..., head_size:], 1, 2)
    local_out = readings[..., :head_size]
    carried_dir = readings[..., head_size:]
    neutral = (identity[:local_attender_number], jnp.zeros_like(identity[:local_attender_number]))
    enter_fwd = carried_in(
        (prod_end[:local_attender_number], state_end[:local_attender_number]),
        SP,
        chain_blocks,
        neutral,
        False,
    )[1]
    enter_bwd = carried_in(
        (prod_end[local_attender_number:], state_end[local_attender_number:]),
        SP,
        chain_blocks,
        neutral,
        True,
    )[1]
    entering = jnp.concatenate([enter_fwd, enter_bwd], axis=0)
    complete = local_out + jnp.einsum("hij,thj->thi", entering, carried_dir)
    summed = complete[:, :local_attender_number] + jnp.flip(complete[:, local_attender_number:], 0)
    center = jnp.mean(summed, -1, keepdims=True)
    spread = jnp.mean(jnp.square(summed - center), -1, keepdims=True)
    rescaled_lines = (
        (summed - center) * lax.rsqrt(spread + GROUP_EPS) * split_attenders(attender_scaling_vector)
    )
    present_reward_summand = (
        jnp.sum(
            entire_asking_lines
            * (stored_label_lines[0] + stored_label_lines[1])
            * split_attenders(present_reward_factors),
            -1,
            keepdims=True,
        )
        * payload_line_slab
    )
    merged_attender_lines = (
        (rescaled_lines + present_reward_summand)
        * split_attenders(blender_result_valve.astype(jnp.float32))
    ).reshape(tok_rows, -1)
    merged_attender_lines = merged_attender_lines.astype(jnp.bfloat16)
    picked = merged_attender_lines
    mixsum = sent_and_summed(
        jnp.dot(picked, blender_result_projector, preferred_element_type=jnp.float32).astype(
            jnp.bfloat16
        ),
        "tp",
        0,
    )
    residual = lax.dynamic_slice_in_dim(skip_stream_entering, row_start, row_share, 0).astype(
        jnp.float32
    )
    middle = layer_norm(RESIDUAL_SCALE * residual + mixsum, blender_scaling_vector).astype(
        jnp.bfloat16
    )
    all_middle = gathered_copies(middle, "tp", 0)
    gate_pre = jnp.dot(all_middle, whole_gate, preferred_element_type=jnp.float32)
    up_pre = jnp.dot(all_middle, whole_up, preferred_element_type=jnp.float32)
    inner_act = (jax.nn.silu(gate_pre) * up_pre).astype(jnp.bfloat16)
    picked = inner_act
    downsum = sent_and_summed(
        jnp.dot(picked, whole_down, preferred_element_type=jnp.float32).astype(jnp.bfloat16),
        "tp",
        0,
    )
    return layer_norm(
        RESIDUAL_SCALE * middle.astype(jnp.float32) + downsum, closing_scaling_vector
    ).astype(jnp.bfloat16)


def solution(mesh):
    finer = Mesh(mesh.devices.reshape(8, 8, mesh.shape["tp"]), ("sp_0", "sp_1", "tp"))
    placed = (
        P(SP, None),
        P(SP, "tp"),
        P(SP, "tp"),
        P(SP, "tp"),
        P(SP, "tp"),
        P(None, SP, "tp"),
        P(None, SP, "tp"),
        P(None, "tp", SP),
        P("tp"),
        P("tp"),
        P("tp", None),
        P(),
        P(SP, "tp"),
        P(SP, "tp"),
        P("tp", SP),
        P(),
    )
    return jax.shard_map(
        shards, mesh=finer, in_specs=placed, out_specs=P(SP_TP, None), check_vma=False
    )
```

profile of v0, /device:TPU:1, one launch (start us, length us, event | category | flops | bytes accessed | tf_op | source)
XLA Modules:
  0.0 250.0 jit_solution(18129958228404149281)
XLA Ops:
  6.5 1.7 concatenate.86
  8.3 0.8 reshape.622
  9.1 0.8 concatenate.78
  10.0 0.8 reshape.637
  11.1 0.8 add_divide_fusion
  12.3 0.8 fusion.136
  13.2 0.8 copy.63
  14.3 0.8 reshape.639
  15.7 61.7 %while.12 = (s32[]{:T(128)}, f32[4,64,128]{2,1,0:T(8,128)S(1)}, f32[4,16,4,128]{3,1,0,2:T(8,128)S(1)}, f32[4,16,4,64]{3,2,1,0:T(4,128)S(1)}, f32[4,16,4,64]{3,2,...) while((s32[]{:T(128)}, f32[4,64,128]{2,1,0:T(8,128)S(1)}, ...), condition=%wide.region_2.3_spmd, body=%wide.region_1.2_spmd.sunk | while | flops 16515089 | bytes 6333085 | solution.py:187
  17.0 0.5 fusion.553
  18.7 0.5 fusion.557
  19.2 0.9 multiply_add_fusion.103
  21.0 0.5 fusion.561
  21.4 1.3 multiply_add_fusion.104
  23.5 0.5 fusion.580
  24.7 0.5 fusion.576
  25.9 0.5 fusion.572
  27.7 0.5 fusion.568
  28.8 0.5 fusion.565
  29.2 1.8 multiply_add_fusion.105
  32.4 0.5 fusion.553
  34.2 0.5 fusion.557
  34.7 0.9 multiply_add_fusion.103
  36.9 1.3 multiply_add_fusion.104
  39.0 0.5 fusion.580
  41.3 0.5 fusion.572
  43.2 0.5 fusion.568
  44.2 0.5 fusion.565
  44.7 1.8 multiply_add_fusion.105
  47.8 0.5 fusion.553
  49.6 0.5 fusion.557
  50.1 0.9 multiply_add_fusion.103
  51.8 0.5 fusion.561
  52.3 1.3 multiply_add_fusion.104
  56.8 0.5 fusion.572
  58.6 0.5 fusion.568
  59.6 0.5 fusion.565
  60.1 1.8 multiply_add_fusion.105
  63.3 0.5 fusion.553
  65.0 0.5 fusion.557
  65.5 0.9 multiply_add_fusion.103
  67.3 0.5 fusion.561
  67.8 1.3 multiply_add_fusion.104
  69.8 0.5 fusion.580
  71.0 0.5 fusion.576
  72.2 0.5 fusion.572
  74.0 0.5 fusion.568
  75.1 0.5 fusion.565
  75.5 1.8 multiply_add_fusion.105
  77.9 25.0 %all-gather = bf16[2048,64]{0,1:T(8,128)(2,1)S(1)} all-gather(bf16[256,64]{0,1:T(8,128)(2,1)S(1)} %pad_maximum_fusion.8), channel_id=2, replica_groups=mesh['sp_0'=8,'sp_1'=8,'tp'=8] {'sp_1'}, dimensions={0}, use_global_device_ids=true | all-gather | bytes 294912 | tf_op jit(solution)/shard_map/all_gather | solution.py:45
  103.5 22.1 %all-gather.2 = bf16[2048,64]{0,1:T(8,128)(2,1)S(1)} all-gather(bf16[256,64]{0,1:T(8,128)(2,1)S(1)} %pad_maximum_fusion.9), channel_id=4, replica_groups=mesh['sp_0'=8,'sp_1'=8,'tp'=8] {'sp_1'}, dimensions={0}, use_global_device_ids=true | all-gather | bytes 294912 | tf_op jit(solution)/shard_map/all_gather | solution.py:45
  130.3 24.4 %all-gather.1 = bf16[2048,64]{1,0:T(8,128)(2,1)S(1)} all-gather(bf16[256,64]{1,0:T(8,128)(2,1)S(1)} %pad_maximum_fusion.6), channel_id=3, replica_groups=mesh['sp_0'=8,'sp_1'=8,'tp'=8] {'sp_0'}, dimensions={0}, use_global_device_ids=true | all-gather | bytes 294912 | tf_op jit(solution)/shard_map/all_gather | solution.py:45
  154.7 19.6 %all-gather.3 = bf16[2048,64]{1,0:T(8,128)(2,1)S(1)} all-gather(bf16[256,64]{1,0:T(8,128)(2,1)S(1)} %pad_maximum_fusion.7), channel_id=5, replica_groups=mesh['sp_0'=8,'sp_1'=8,'tp'=8] {'sp_0'}, dimensions={0}, use_global_device_ids=true | all-gather | bytes 294912 | tf_op jit(solution)/shard_map/all_gather | solution.py:45
  178.7 0.9 fusion.97
  179.7 25.6 %all-to-all-start = ((bf16[8,8,2048]{2,1,0:T(8,128)(2,1)}), bf16[8,8,2048]{2,1,0:T(8,128)(2,1)S(1)}, u32[]{:S(2)}, u32[]{:S(2)}) async-start(bf16[8,8,2048]{2,1,0:T(8,128)(2,1)} %fusion.97), calls=%async_computation | async-start | bytes 524288 | tf_op jit(solution)/shard_map/all_to_all | solution.py:81
  205.3 6.5 %all-to-all-done = bf16[8,8,2048]{2,1,0:T(8,128)(2,1)S(1)} async-done(((bf16[8,8,2048]{2,1,0:T(8,128)(2,1)}), bf16[8,8,2048]{2,1,0:T(8,128)(2,1)S(1)}, u32[]{:S(2)}, u32[]{:S(2)}) %all-to-all-start) | async-done | bytes 262176 | tf_op jit(solution)/shard_map/all_to_all | solution.py:81
  211.8 0.9 fusion.256
  212.7 1.0 multiply_reduce_fusion.1
  213.7 0.8 multiply_convert_fusion.1
  214.6 9.9 %all_to_all.15 = bf16[8,8,2048]{2,1,0:T(8,128)(2,1)S(1)} all-to-all(bf16[8,8,2048]{2,1,0:T(8,128)(2,1)S(1)} %broadcast_in_dim.79), channel_id=1, replica_groups=mesh['sp_0'=8,'sp_1'=8,'tp'=8] {'tp'}, dimensions={0} | all-to-all | bytes 524288 | tf_op jit(solution)/shard_map/all_to_all | solution.py:93
  224.5 2.5 %fusion.92 = f32[64,704]{1,0:T(8,128)S(1)} fusion(bf16[2048,2112]{1,0:T(8,128)(2,1)} %all-gather.6.cloned.1.call-done, bf16[8,8,2048]{2,1,0:T(8,128)(2,1)S(1)} %all_to_all.15), kind=kOutput, calls=%fused_computation.221 | convolution fusion | flops 184549376 | bytes 3588096 | tf_op jit(solution)/shard_map/dot_general | solution.py:245
  227.0 5.2 %fusion.98 = bf16[8,8,2048]{2,1,0:T(8,128)(2,1)S(1)} fusion(bf16[2048,2112]{1,0:T(8,128)(2,1)} %all-gather.6.cloned.1.call-done, bf16[8,8,2048]{2,1,0:T(8,128)(2,1)S(1)} %all_to_all.15, f32[64,704]{1,0:T(8,128)S(1)} %fusion.92), kind=kOutput, calls=%fused_computation.226 | convolution fusion | flops 369500160 | bytes 6995968 | tf_op jit(solution)/shard_map/dot_general | solution.py:250
  232.2 9.9 %all_to_all.16 = bf16[8,8,2048]{2,1,0:T(8,128)(2,1)S(1)} all-to-all(bf16[8,8,2048]{2,1,0:T(8,128)(2,1)S(1)} %fusion.98), channel_id=1, replica_groups=mesh['sp_0'=8,'sp_1'=8,'tp'=8] {'tp'}, dimensions={0} | all-to-all | bytes 524288 | tf_op jit(solution)/shard_map/all_to_all | solution.py:81
  242.5 0.7 multiply_convert_fusion
  (325 shorter events, 43.5 us)
Async XLA Ops:
  6.5 172.2 %copy-start = (bf16[128,2048]{1,0:T(8,128)(2,1)S(1)}, bf16[128,2048]{1,0:T(8,128)(2,1)}, u32[]{:S(2)}) copy-start(bf16[128,2048]{1,0:T(8,128)(2,1)} %param.28) | copy-start | bytes 1572868
  6.5 217.9 %all-gather.6.cloned.1.call-start = ((), (), s32[]{:S(2)}) async-start(), calls=%async_computation.3 | async-start | bytes 9052160 | tf_op jit(solution)/shard_map/all_gather | solution.py:21
  77.5 100.2 %copy-start.4 = (f32[128]{0:T(128)S(1)}, f32[128]{0:T(128)}, u32[]{:S(2)}) copy-start(f32[128]{0:T(128)} %param.26) | copy-start | bytes 1540
  77.6 100.4 %copy-start.1 = (bf16[64,128]{1,0:T(8,128)(2,1)S(1)}, bf16[64,128]{1,0:T(8,128)(2,1)}, u32[]{:S(2)}) copy-start(bf16[64,128]{1,0:T(8,128)(2,1)} %param.22) | copy-start | bytes 49156
  77.6 100.5 %copy-start.5 = (f32[128]{0:T(128)S(1)}, f32[128]{0:T(128)}, u32[]{:S(2)}) copy-start(f32[128]{0:T(128)} %param.27) | copy-start | bytes 1540
  125.6 88.1 %copy-start.2 = (f32[2048]{0:T(1024)S(1)}, f32[2048]{0:T(1024)}, u32[]{:S(2)}) copy-start(f32[2048]{0:T(1024)} %param.29) | copy-start | bytes 24580
  177.4 65.1 %copy-start.3 = (f32[2048]{0:T(1024)S(1)}, f32[2048]{0:T(1024)}, u32[]{:S(2)}) copy-start(f32[2048]{0:T(1024)} %param.33) | copy-start | bytes 24580
  179.7 32.1 %all-to-all-start = ((bf16[8,8,2048]{2,1,0:T(8,128)(2,1)}), bf16[8,8,2048]{2,1,0:T(8,128)(2,1)S(1)}, u32[]{:S(2)}, u32[]{:S(2)}) async-start(bf16[8,8,2048]{2,1,0:T(8,128)(2,1)} %fusion.97), calls=%async_computation | async-start | bytes 524288 | tf_op jit(solution)/shard_map/all_to_all | solution.py:81
Sparse Core Ops, SparseCore 0:
  10.3 110.1 all-gather.5
where the time goes:
time: 251 us; the launch traced here: 250 us
  blocking collectives  111 us (44%)
  matrix products  57.5 us (23%)
  starting transfers between devices  25.6 us (10%)
  other arithmetic  24.8 us (10%)
  between operations  14.1 us (6%)
  local copies, waits for them, and re-layouts  10.3 us (4%)
  waiting for transfers between devices  6.49 us (3%)
    all_gather x4, blocking collectives, collected_together(): both, at, found = (lax.all_gather(jnp.concatenate(lines), axis), 0, {})  91.1 us
    all_to_all x1, starting transfers between devices, sent_and_summed(): lax.all_to_all(cut_along(value, dim, length), axis, 0, 0, tiled=True)  25.6 us
    dot_general x64, matrix products, advance(): return (joined, jnp.einsum('hji,hj->hi', joined, query_vec))  20.8 us
    dot_general x64, matrix products, advance(): erased = jnp.einsum('hji,hj->hi', joined, erase_vec)  20.7 us
    add x16, other arithmetic, advance(): joined * decay_vec[:, :, None] + refill_vec[:, :, None] * erased[:, None, :]  17.8 us
    all_to_all x1, blocking collectives, sent_to_all(): return lax.all_to_all(copies, axis, split_axis=0, concat_axis=0, tiled=True)  9.91 us
    all_to_all x1, blocking collectives, sent_and_summed(): lax.all_to_all(cut_along(value, dim, length), axis, 0, 0, tiled=True)  9.91 us
    all_to_all x1, waiting for transfers between devices, sent_and_summed(): lax.all_to_all(cut_along(value, dim, length), axis, 0, 0, tiled=True)  6.47 us
  transfers between devices with their start and end apart: 2, of which 1 were waited for; matrix products, arithmetic and copies ran while one was open for 33% of the time, Pallas kernels for 0%

commit v1 on v0

v1 whole, which is shorter than its diff:
```python
import functools
import math

import jax
import jax.numpy as jnp
from jax import lax
from jax.experimental import pallas as pl
from jax.experimental.pallas import tpu as pltpu
from jax.sharding import Mesh
from jax.sharding import PartitionSpec as P

Y = ("yh", "yl")
SP = ("z", "yh", "yl")
SP_TP = ("z", "yh", "yl", "tp")
PEERS = ("yl", "tp")

RESIDUAL_SCALE = 2.0**0.25
NORM_EPS = 1e-05
GROUP_EPS = 0.00064
KEY_EPS = 1e-06
TOK = 64
HEAD = 64
WIDE = 128
SUB = 16
UNITS = 704
PART = 384
D = 2048
F32 = jnp.float32
BF16 = jnp.bfloat16


def iota(shape, dim):
    return lax.broadcasted_iota(jnp.int32, shape, dim)


def dot(a, b):
    return jnp.dot(a, b, preferred_element_type=F32, precision=lax.Precision.HIGHEST)


def dot_nt(a, b):
    return lax.dot_general(
        a, b, (((1,), (1,)), ((), ())), preferred_element_type=F32, precision=lax.Precision.HIGHEST
    )


def dot_tn(a, b):
    return lax.dot_general(
        a, b, (((0,), (0,)), ((), ())), preferred_element_type=F32, precision=lax.Precision.HIGHEST
    )


def low_half(shape):
    return (iota(shape, len(shape) - 1) % WIDE) < HEAD


def by_head(x):
    low = low_half(x.shape)
    return jnp.concatenate([jnp.where(low, x, 0.0), jnp.where(low, 0.0, x)], axis=0)


def joined_heads(x):
    return x[:HEAD] + x[HEAD:]


def head_ones():
    return ((iota((WIDE, WIDE), 0) // HEAD) == (iota((WIDE, WIDE), 1) // HEAD)).astype(F32)


def head_eye():
    return (iota((HEAD, WIDE), 0) == iota((HEAD, WIDE), 1) % HEAD).astype(F32)


def sigmoid(x):
    return 1.0 / (1.0 + jnp.exp(-x))


def unit_lower_inverse(a):
    row, col = iota((WIDE, WIDE), 0), iota((WIDE, WIDE), 1)
    eye = (row == col).astype(F32)
    near = jnp.where(row // 8 == col // 8, a, 0.0)
    second = dot(near, near)
    fourth = dot(second, second)
    inverse = eye - near + second - dot(near, second)
    inverse = inverse + dot(inverse, fourth)
    for size in (8, 16, 32):
        across = (row // (2 * size) == col // (2 * size)) & (row // size != col // size)
        inverse = inverse - dot(inverse, dot(jnp.where(across, a, 0.0), inverse))
    return inverse


def one_way(back, reads, unit, keys, values, log_decay, rate):
    refill, write = unit * rate, keys * rate
    row, col = iota((TOK, TOK), 0), iota((TOK, TOK), 1)
    reach = (col >= row) if back else (col <= row)
    upto = dot(reach.astype(F32), log_decay)
    ahead = upto - log_decay
    whole = upto[:1] if back else upto[TOK - 1 :]
    low = low_half((SUB, WIDE))
    first, second = [], []
    for block in range(TOK // SUB):
        rows = slice(block * SUB, (block + 1) * SUB)
        edge = (block + 1) * SUB - 1 if back else block * SUB
        start = ahead[edge : edge + 1]
        scale = jnp.exp(jnp.minimum(start - upto, 60.0))
        erase_keys, write_keys = refill * scale, write * scale
        erased = unit[rows] * jnp.exp(ahead[rows] - start)
        read = reads[rows] * jnp.exp(upto[rows] - start)
        first.append(
            dot_nt(
                jnp.concatenate([jnp.where(low, erased, 0.0), jnp.where(low, read, 0.0)], axis=0),
                jnp.concatenate([erase_keys, write_keys], axis=0),
            )
        )
        second.append(
            dot_nt(
                jnp.concatenate([jnp.where(low, 0.0, erased), jnp.where(low, 0.0, read)], axis=0),
                jnp.concatenate([write_keys, erase_keys], axis=0),
            )
        )
    row, col = iota((TOK, WIDE), 0), iota((TOK, WIDE), 1) % HEAD
    past = (col > row) if back else (col < row)
    seen = (col >= row) if back else (col <= row)
    low = low_half((TOK, WIDE))

    def pieces(kept, lo):
        one = jnp.concatenate([part[lo : lo + SUB] for part in first], axis=0)
        two = jnp.concatenate([part[lo : lo + SUB] for part in second], axis=0)
        one, two = jnp.where(kept, one, 0.0), jnp.where(kept, two, 0.0)
        same = jnp.concatenate([jnp.where(low, one, 0.0), jnp.where(low, 0.0, two)], axis=0)
        other = jnp.concatenate([jnp.where(low, 0.0, one), jnp.where(low, two, 0.0)], axis=0)
        return same, other

    erase_erase, erase_write = pieces(past, 0)
    read_erase, read_write = pieces(seen, SUB)
    straight = by_head(values)
    crossed = jnp.concatenate([straight[TOK:], straight[:TOK]], axis=0)
    asked = jnp.concatenate([dot(erase_write, crossed), by_head(unit * jnp.exp(ahead))], axis=1)
    erased = -dot(unit_lower_inverse(erase_erase), asked)
    out = dot(read_erase, erased) + jnp.concatenate(
        [dot(read_write, crossed), by_head(reads * jnp.exp(upto))], axis=1
    )
    left = jnp.exp(whole - upto)
    state = dot_tn(by_head(refill * left), erased)
    state = joined_heads(state) + jnp.concatenate(
        [
            joined_heads(dot_tn(by_head(write * left), straight)),
            head_eye() * jnp.exp(whole),
        ],
        axis=1,
    )
    return joined_heads(out), state


def mixer_local(reads_ref, keys_ref, values_ref, fades_ref, rates_ref, extra_ref, send_ref, out_ref):
    reads, keys = reads_ref[...].astype(F32), keys_ref[...].astype(F32)
    values = values_ref[...].astype(F32)
    unit = keys * lax.rsqrt(dot(keys * keys, head_ones()) + KEY_EPS)
    lanes_of = (iota((2, WIDE), 1) // HEAD == iota((2, WIDE), 0)).astype(F32)
    for way in range(2):
        log_decay = -math.exp(-0.5) * sigmoid(fades_ref[way].astype(F32)) + dot_tn(
            extra_ref[way], lanes_of
        )
        rate = sigmoid(rates_ref[way].astype(F32))
        out, state = one_way(way == 1, reads, unit, keys, values, log_decay, rate)
        out_ref[way] = out
        state = state.astype(BF16)
        for peer in range(send_ref.shape[0]):
            send_ref[peer, :, way * 2 * WIDE : (way + 1) * 2 * WIDE] = state


def advanced(piece, running):
    moved = dot(piece[:, WIDE:], by_head(running))
    if running.shape[1] == WIDE:
        return moved + piece[:, :WIDE]
    return moved + jnp.concatenate([piece[:, :WIDE], jnp.zeros((HEAD, WIDE), F32)], axis=1)


def combine_near(place_ref, got_ref, send_ref, pre_ref):
    y, z = place_ref[0], place_ref[1]
    start = jnp.concatenate([jnp.zeros((HEAD, WIDE), F32), head_eye()], axis=1)
    total, before = [start, start], [start, start]
    for step in range(8):
        for way in range(2):
            k = 7 - step if way else step
            piece = got_ref[k, :, way * 2 * WIDE : (way + 1) * 2 * WIDE].astype(F32)
            total[way] = advanced(piece, total[way])
            passed = (k > y) if way else (k < y)
            before[way] = jnp.where(passed, total[way], before[way])
    for way in range(2):
        pre_ref[way] = before[way]
    ahead, behind = total[0].astype(BF16), total[1].astype(BF16)
    for peer in range(8):
        send_ref[peer] = jnp.where(peer > z, ahead, behind)


def finish_mixer(
    place_ref,
    got_ref,
    pre_ref,
    local_ref,
    reads_ref,
    keys_ref,
    values_ref,
    rates_ref,
    valve_ref,
    reward_ref,
    gain_ref,
    projector_ref,
    send_ref,
):
    z = place_ref[1]
    state = [jnp.zeros((HEAD, WIDE), F32)] * 2
    for step in range(8):
        for way in range(2):
            k = 7 - step if way else step
            passed = (k > z) if way else (k < z)
            state[way] = jnp.where(
                passed, advanced(got_ref[k].astype(F32), state[way]), state[way]
            )
    summed = 0.0
    for way in range(2):
        entering = advanced(pre_ref[way], state[way])
        summed = summed + local_ref[way, :, :WIDE]
        summed = summed + dot(local_ref[way, :, WIDE:], by_head(entering))
    ones = head_ones()
    off = summed - dot(summed, ones) * (1.0 / HEAD)
    spread = dot(off * off, ones) * (1.0 / HEAD)
    normed = off * lax.rsqrt(spread + GROUP_EPS) * gain_ref[...]
    keys = keys_ref[...].astype(F32)
    both = keys * sigmoid(rates_ref[0].astype(F32)) + keys * sigmoid(rates_ref[1].astype(F32))
    bonus = dot(reads_ref[...].astype(F32) * both * reward_ref[...], ones)
    bonus = bonus * values_ref[...].astype(F32)
    mixed = ((normed + bonus) * valve_ref[...].astype(F32)).astype(BF16)
    share = jnp.dot(mixed, projector_ref[...], preferred_element_type=F32)
    send_ref[...] = share.astype(BF16).reshape(send_ref.shape)


def normed_rows(x, gain):
    off = x - jnp.mean(x, axis=-1, keepdims=True)
    spread = jnp.mean(off * off, axis=-1, keepdims=True)
    return off * lax.rsqrt(spread + NORM_EPS) * gain


def middle_rows(place_ref, got_ref, skip_ref, gain_ref, send_ref):
    summed = jnp.sum(got_ref[...].astype(F32), axis=0)
    summed = summed + RESIDUAL_SCALE * skip_ref[...].astype(F32)
    middle = normed_rows(summed, gain_ref[...]).astype(BF16)
    for peer in range(send_ref.shape[0]):
        send_ref[peer] = middle


def closing_rows(got_ref, middle_ref, gain_ref, out_ref):
    summed = jnp.sum(got_ref[...].astype(F32), axis=0)
    summed = summed + RESIDUAL_SCALE * middle_ref[0].astype(F32)
    out_ref[...] = normed_rows(summed, gain_ref[...]).astype(BF16)


def pack_weights(valve_ref, widen_ref, shrink_ref, send_ref):
    rows = valve_ref.shape[0]
    eye = (iota((rows, rows), 0) == iota((rows, rows), 1)).astype(BF16)
    turned = lax.dot_general(
        eye, shrink_ref[...], (((1,), (1,)), ((), ())), preferred_element_type=F32
    ).astype(BF16)
    blank = jnp.zeros((rows, 2 * PART - UNITS), BF16)
    halves = []
    for lo in (0, PART):
        line = []
        for whole in (valve_ref[...], widen_ref[...], turned):
            line.append(whole[:, lo : lo + PART])
            if lo:
                line.append(blank)
        halves.append(jnp.concatenate(line, axis=1))
    for peer in range(send_ref.shape[0]):
        send_ref[peer] = halves[peer % 2]


CHUNK = 1024
STEPS = D // CHUNK


def feed_forward(rows_ref, up_ref, down_ref, out_ref, acc_ref, inner_ref):
    step = pl.program_id(0)

    @pl.when(step < STEPS)
    def _():
        at = pl.multiple_of(step * CHUNK, CHUNK)
        part = jnp.dot(rows_ref[:, pl.ds(at, CHUNK)], up_ref[...], preferred_element_type=F32)
        acc_ref[...] = jnp.where(step == 0, part, acc_ref[...] + part)

    @pl.when(step == STEPS - 1)
    def _():
        gate, up = acc_ref[:, :PART], acc_ref[:, PART:]
        inner_ref[...] = (gate / (1.0 + jnp.exp(-gate)) * up).astype(BF16)

    @pl.when(step >= STEPS)
    def _():
        share = lax.dot_general(
            inner_ref[...], down_ref[...], (((1,), (1,)), ((), ())), preferred_element_type=F32
        )
        out_ref[...] = share.astype(BF16).reshape(out_ref.shape)


VMEM = pl.BlockSpec(memory_space=pltpu.VMEM)
SMEM = pl.BlockSpec(memory_space=pltpu.SMEM)


def shape(dims, kind=BF16):
    return jax.ShapeDtypeStruct(dims, kind)


def exchanged(value, axis):
    return lax.all_to_all(value, axis, 0, 0, tiled=True)


def run_mixer_local(*args):
    return pl.pallas_call(
        mixer_local,
        in_specs=[VMEM] * 6,
        out_specs=[VMEM] * 2,
        out_shape=[shape((8, HEAD, 4 * WIDE)), shape((2, TOK, 2 * WIDE), F32)],
        name="mixer_local",
    )(*args)


def run_combine_near(place, got):
    return pl.pallas_call(
        combine_near,
        in_specs=[SMEM, VMEM],
        out_specs=[VMEM] * 2,
        out_shape=[shape((8, HEAD, 2 * WIDE)), shape((2, HEAD, 2 * WIDE), F32)],
        name="combine_near",
    )(place, got)


def run_finish_mixer(place, *args):
    return pl.pallas_call(
        finish_mixer,
        in_specs=[SMEM] + [VMEM] * (len(args)),
        out_specs=VMEM,
        out_shape=shape((8, 8, D)),
        name="finish_mixer",
    )(place, *args)


def run_middle_rows(place, got, skip, gain, peers):
    return pl.pallas_call(
        middle_rows,
        grid_spec=pltpu.PrefetchScalarGridSpec(
            num_scalar_prefetch=1,
            grid=(1,),
            in_specs=[
                pl.BlockSpec((8, 8, D), lambda i, place: (0, 0, 0)),
                pl.BlockSpec((8, D), lambda i, place: (place[2], 0)),
                pl.BlockSpec((1, D), lambda i, place: (0, 0)),
            ],
            out_specs=pl.BlockSpec((peers, 8, D), lambda i, place: (0, 0, 0)),
        ),
        out_shape=shape((peers, 8, D)),
        name="middle_rows",
    )(place, got, skip, gain)


def run_feed_forward(rows, weights, peers):
    return pl.pallas_call(
        feed_forward,
        grid=(2 * STEPS,),
        in_specs=[
            pl.BlockSpec((peers * 8, D), lambda i: (0, 0)),
            pl.BlockSpec((CHUNK, 2 * PART), lambda i: (jnp.minimum(i, STEPS - 1), 0)),
            pl.BlockSpec((CHUNK, PART), lambda i: (jnp.maximum(i - STEPS, 0), 2)),
        ],
        out_specs=pl.BlockSpec((peers, 8, CHUNK), lambda i: (0, 0, jnp.maximum(i - STEPS, 0))),
        out_shape=shape((peers, 8, D)),
        scratch_shapes=[
            pltpu.VMEM((peers * 8, 2 * PART), F32),
            pltpu.VMEM((peers * 8, PART), BF16),
        ],
        name="feed_forward",
    )(rows, weights, weights)


def run_closing_rows(got, middle, gain):
    return pl.pallas_call(
        closing_rows,
        grid=(1,),
        in_specs=[
            pl.BlockSpec(got.shape, lambda i: (0, 0, 0)),
            pl.BlockSpec((1, 8, D), lambda i: (0, 0, 0)),
            pl.BlockSpec((1, D), lambda i: (0, 0)),
        ],
        out_specs=pl.BlockSpec((8, D), lambda i: (0, 0)),
        out_shape=shape((8, D)),
        name="closing_rows",
    )(got, middle, gain)


def shards(
    skip_stream_entering,
    reading_vectors,
    blender_lookup_labels,
    blender_payloads,
    blender_result_valve,
    fading_logits,
    amend_speed_logits,
    extra_log_fades,
    present_reward_factors,
    attender_scaling_vector,
    blender_result_projector,
    blender_scaling_vector,
    perceptron_valve_factors,
    perceptron_widen_factors,
    perceptron_shrink_factors,
    closing_scaling_vector,
):
    place = jnp.stack([lax.axis_index(Y), lax.axis_index("z"), lax.axis_index("tp")]).astype(
        jnp.int32
    )
    packed = pl.pallas_call(
        pack_weights,
        in_specs=[VMEM] * 3,
        out_specs=VMEM,
        out_shape=shape((8, 32, 3 * PART)),
        name="pack_weights",
    )(perceptron_valve_factors, perceptron_widen_factors, perceptron_shrink_factors)
    near_weights = exchanged(packed, Y).reshape(256, 3 * PART)
    weights = lax.all_gather(near_weights, "z", axis=0, tiled=True)

    sends, local = run_mixer_local(
        reading_vectors,
        blender_lookup_labels,
        blender_payloads,
        fading_logits,
        amend_speed_logits,
        extra_log_fades,
    )
    totals, before = run_combine_near(place, exchanged(sends, Y))
    shares = run_finish_mixer(
        place,
        exchanged(totals, "z"),
        before,
        local,
        reading_vectors,
        blender_lookup_labels,
        blender_payloads,
        amend_speed_logits,
        blender_result_valve,
        present_reward_factors.reshape(1, WIDE),
        attender_scaling_vector.reshape(1, WIDE),
        blender_result_projector,
    )
    peers = 16
    middle = run_middle_rows(
        place, exchanged(shares, "tp"), skip_stream_entering, blender_scaling_vector.reshape(1, D), peers
    )
    rows = exchanged(middle, PEERS).reshape(peers * 8, D)
    down = run_feed_forward(rows, weights, peers)
    return run_closing_rows(exchanged(down, PEERS), middle, closing_scaling_vector.reshape(1, D))


def solution(mesh):
    finer = Mesh(mesh.devices.reshape(8, 4, 2, mesh.shape["tp"]), SP_TP)
    placed = (
        P(SP, None),
        P(SP, "tp"),
        P(SP, "tp"),
        P(SP, "tp"),
        P(SP, "tp"),
        P(None, SP, "tp"),
        P(None, SP, "tp"),
        P(None, "tp", SP),
        P("tp"),
        P("tp"),
        P("tp", None),
        P(),
        P(SP, "tp"),
        P(SP, "tp"),
        P("tp", SP),
        P(),
    )
    return jax.shard_map(
        shards, mesh=finer, in_specs=placed, out_specs=P(SP_TP, None), check_vma=False
    )
```

time: 251 us -> 159 us (0.63)
  matrix products: 57.5 us -> 0 us
  Pallas kernels: 0 us -> 30.1 us
  other arithmetic: 24.8 us -> 0.65 us
  starting transfers between devices: 25.6 us -> 4.02 us
  blocking collectives: 111 us -> 96.9 us
  local copies, waits for them, and re-layouts: 10.3 us -> 2.43 us
  waiting for transfers between devices: 6.49 us -> 11 us
    all_gather x4 -> x0, blocking collectives: 91.1 us -> none  [collected_together(): both, at, found = (lax.all_gather(jnp.concatenate(lines), axis), 0, {})]
    all_to_all x2 -> x5, blocking collectives: 19.8 us -> 96.9 us  [exchanged(): return lax.all_to_all(value, axis, 0, 0, tiled=True)]
    dot_general x184 -> x0, matrix products: 57.5 us -> none  [the longest x64 20.8 us: advance(): return (joined, jnp.einsum('hji,hj->hi', joined, query_vec))]
    pallas_call x0 -> x7, Pallas kernels: none -> 30.1 us  [the longest x1 9.74 us: run_mixer_local(): pl.pallas_call(mixer_local, in_specs=[VMEM] * 6, out_specs=[VMEM] * 2, ou...]
    all_to_all x1, starting transfers between devices: 25.6 us -> 4.02 us  [exchanged(): return lax.all_to_all(value, axis, 0, 0, tiled=True)]
    add x16 -> x0, other arithmetic: 17.8 us -> none  [advance(): joined * decay_vec[:, :, None] + refill_vec[:, :, None] * erased[:, None, :]]
    all_to_all x1, waiting for transfers between devices: 6.47 us -> 11 us  [exchanged(): return lax.all_to_all(value, axis, 0, 0, tiled=True)]
    reduce_sum x10 -> x0, other arithmetic: 2.81 us -> none  [the longest x2 1.16 us: layer_norm(): spread = jnp.mean(jnp.square(summand - center), -1, keepdims=True)]
  transfers between devices with their start and end apart: 2 -> 2, of which waited for: 1 -> 1; matrix products, arithmetic and copies ran while one was open for 33% -> 0% of each run, Pallas kernels for 0% -> 13%
where the time goes in v1:
time: 159 us
  blocking collectives  96.9 us (61%)
  Pallas kernels  30.1 us (19%)
  between operations  13.4 us (8%)
  waiting for transfers between devices  11 us (7%)
  starting transfers between devices  4.02 us (3%)
  local copies, waits for them, and re-layouts  2.43 us (2%)
    all_to_all x5, blocking collectives, exchanged(): return lax.all_to_all(value, axis, 0, 0, tiled=True)  96.9 us
    all_to_all x1, waiting for transfers between devices, exchanged(): return lax.all_to_all(value, axis, 0, 0, tiled=True)  11 us
    pallas_call x1, Pallas kernels, run_mixer_local(): pl.pallas_call(mixer_local, in_specs=[VMEM] * 6, out_specs=[VMEM] * 2, ou...  9.74 us
    pallas_call x1, Pallas kernels, run_finish_mixer(): pl.pallas_call(finish_mixer, in_specs=[SMEM] + [VMEM] * len(args), out_sp...  5.1 us
    pallas_call x1, Pallas kernels, run_feed_forward(): pl.pallas_call(feed_forward, grid=(2 * STEPS,), in_specs=[pl.BlockSpec((p...  4.98 us
    all_to_all x1, starting transfers between devices, exchanged(): return lax.all_to_all(value, axis, 0, 0, tiled=True)  4.02 us
    pallas_call x1, Pallas kernels, run_combine_near(): pl.pallas_call(combine_near, in_specs=[SMEM, VMEM], out_specs=[VMEM] * 2,...  3.64 us
  transfers between devices with their start and end apart: 2, of which 1 were waited for; matrix products, arithmetic and copies ran while one was open for 0% of the time, Pallas kernels for 13%

profile of v1, /device:TPU:1, one launch (start us, length us, event | category | flops | bytes accessed | tf_op | source)
XLA Modules:
  0.0 158.5 jit_solution(18348328078168670475)
XLA Ops:
  6.5 0.0 all-gather.2.cloned.1.call-start
  6.5 1.6 %copy.17.shrink_ref = bf16[704,32]{1,0:T(8,128)(2,1)} copy(bf16[704,32]{0,1:T(8,128)(2,1)} %param.30) | data formatting | bytes 90112 | tf_op args[14]
  8.1 2.0 %pack_weights.1 = bf16[8,32,1152]{2,1,0:T(8,128)(2,1)} custom-call(bf16[32,704]{1,0:T(8,128)(2,1)} %valve_ref.3, bf16[32,704]{1,0:T(8,128)(2,1)} %widen_ref.1, bf16[704,32]{1,0:T(8,128)(2,1)} %copy.17.shrink_ref), custom_call_target="tpu_custom_call" | custom-call | tf_op jit(solution)/shard_map/pack_weights/pallas_call | solution.py:418
  10.1 22.4 %all_to_all.30 = bf16[8,32,1152]{2,1,0:T(8,128)(2,1)} all-to-all(bf16[8,32,1152]{2,1,0:T(8,128)(2,1)} %pack_weights.1), channel_id=1, replica_groups=mesh['z'=8,'yh'=4,'yl'=2,'tp'=8] {'yh','yl'}, dimensions={0} | all-to-all | bytes 1179648 | tf_op jit(solution)/shard_map/all_to_all | solution.py:312
  32.5 0.0 all-gather.2.cloned.1.call-update
  32.5 9.7 %mixer_local.1 = (bf16[8,64,512]{2,1,0:T(8,128)(2,1)}, f32[2,64,256]{2,1,0:T(8,128)}) custom-call(bf16[64,128]{1,0:T(8,128)(2,1)} %reads_ref.3, bf16[64,128]{1,0:T(8,128)(2,1)} %keys_ref.3, bf16[64,128]{1,0:T(8,128)(2,1)} %values_ref.3, bf16[2,64,128]{2,1,0:T(8,128)(2,1)} %fades_ref.1, bf16[2,64,128]{2,1,0:T(8,128)(2,1)} %rates_ref.3, f32[2,2,64]{2,1,0:T(2,128)} %extra_ref.1), custom_call_target="tpu_custom_call" | custom-call | tf_op jit(solution)/shard_map/mixer_local/pallas_call | solution.py:316
  42.3 4.0 %all-to-all-start = ((bf16[8,64,512]{2,1,0:T(8,128)(2,1)}), bf16[8,64,512]{2,1,0:T(8,128)(2,1)S(1)}, u32[]{:S(2)}, u32[]{:S(2)}) async-start(bf16[8,64,512]{2,1,0:T(8,128)(2,1)} %get-tuple-element.9), calls=%async_computation | async-start | bytes 1048576 | tf_op jit(solution)/shard_map/all_to_all | solution.py:312
  46.3 0.7 pad_add_fusion.place_ref
  46.9 11.0 %all-to-all-done.got_ref = bf16[8,64,512]{2,1,0:T(8,128)(2,1)S(1)} async-done(((bf16[8,64,512]{2,1,0:T(8,128)(2,1)}), bf16[8,64,512]{2,1,0:T(8,128)(2,1)S(1)}, u32[]{:S(2)}, u32[]{:S(2)}) %all-to-all-start) | async-done | bytes 524320 | tf_op jit(solution)/shard_map/all_to_all | solution.py:312
  57.9 0.0 copy-start
  57.9 0.8 copy-done
  58.8 3.6 %combine_near.1 = (bf16[8,64,256]{2,1,0:T(8,128)(2,1)}, f32[2,64,256]{2,1,0:T(8,128)}) custom-call(s32[3]{0:T(128)} %pad_add_fusion.place_ref, bf16[8,64,512]{2,1,0:T(8,128)(2,1)} %copy-done), custom_call_target="tpu_custom_call" | custom-call | tf_op jit(solution)/shard_map/combine_near/pallas_call | solution.py:326
  62.4 30.0 %all_to_all.31.got_ref = bf16[8,64,256]{2,1,0:T(8,128)(2,1)} all-to-all(bf16[8,64,256]{2,1,0:T(8,128)(2,1)} %get-tuple-element.10), channel_id=1, replica_groups=mesh['z'=8,'yh'=4,'yl'=2,'tp'=8] {'z'}, dimensions={0} | all-to-all | bytes 524288 | tf_op jit(solution)/shard_map/all_to_all | solution.py:312
  92.4 5.1 %finish_mixer.1 = bf16[8,8,2048]{2,1,0:T(8,128)(2,1)} custom-call(s32[3]{0:T(128)} %pad_add_fusion.place_ref, bf16[8,64,256]{2,1,0:T(8,128)(2,1)} %all_to_all.31.got_ref, f32[2,64,256]{2,1,0:T(8,128)} %get-tuple-element.11.pre_ref, f32[2,64,256]{2,1,0:T(8,128)} %get-tuple-element.12.local_ref, bf16[64,128]{1,0:T(8,128)(2,1)} %reads_ref.3, ...), custom_call_target="tpu_custom_call" | custom-call | tf_op jit(solution)/shard_map/finish_mixer/pallas_call | solution.py:336
  97.5 14.6 %all_to_all.32.got_ref = bf16[8,8,2048]{2,1,0:T(8,128)(2,1)} all-to-all(bf16[8,8,2048]{2,1,0:T(8,128)(2,1)} %finish_mixer.1), channel_id=1, replica_groups=mesh['z'=8,'yh'=4,'yl'=2,'tp'=8] {'tp'}, dimensions={0} | all-to-all | bytes 524288 | tf_op jit(solution)/shard_map/all_to_all | solution.py:312
  112.1 2.7 %middle_rows.1.middle_ref = bf16[16,8,2048]{2,1,0:T(8,128)(2,1)} custom-call(s32[3]{0:T(128)} %pad_add_fusion.place_ref, bf16[8,8,2048]{2,1,0:T(8,128)(2,1)} %all_to_all.32.got_ref, bf16[64,2048]{1,0:T(8,128)(2,1)} %skip_ref.1, f32[1,2048]{1,0:T(1,128)} %bitcast.11), custom_call_target="tpu_custom_call" | custom-call | tf_op jit(solution)/shard_map/middle_rows/pallas_call | solution.py:346
  114.8 14.8 %all_to_all.33 = bf16[16,8,2048]{2,1,0:T(8,128)(2,1)} all-to-all(bf16[16,8,2048]{2,1,0:T(8,128)(2,1)} %middle_rows.1.middle_ref), channel_id=1, replica_groups=mesh['z'=8,'yh'=4,'yl'=2,'tp'=8] {'yl','tp'}, dimensions={0} | all-to-all | bytes 1048576 | tf_op jit(solution)/shard_map/all_to_all | solution.py:312
  129.7 0.0 all-gather.2.cloned.1.call-done.up_ref.down_ref
  129.7 5.0 %feed_forward.1 = bf16[16,8,2048]{2,1,0:T(8,128)(2,1)} custom-call(bf16[128,2048]{1,0:T(8,128)(2,1)} %bitcast.10, bf16[2048,1152]{1,0:T(8,128)(2,1)} %all-gather.2.cloned.1.call-done.up_ref.down_ref, bf16[2048,1152]{1,0:T(8,128)(2,1)} %all-gather.2.cloned.1.call-done.up_ref.down_ref), custom_call_target="tpu_custom_call" | custom-call | tf_op jit(solution)/shard_map/feed_forward/pallas_call | solution.py:364
  134.6 15.1 %all_to_all.34.got_ref = bf16[16,8,2048]{2,1,0:T(8,128)(2,1)} all-to-all(bf16[16,8,2048]{2,1,0:T(8,128)(2,1)} %feed_forward.1), channel_id=1, replica_groups=mesh['z'=8,'yh'=4,'yl'=2,'tp'=8] {'yl','tp'}, dimensions={0} | all-to-all | bytes 1048576 | tf_op jit(solution)/shard_map/all_to_all | solution.py:312
  149.7 2.0 %closing_rows.1 = bf16[8,2048]{1,0:T(8,128)(2,1)} custom-call(bf16[16,8,2048]{2,1,0:T(8,128)(2,1)} %all_to_all.34.got_ref, bf16[16,8,2048]{2,1,0:T(8,128)(2,1)} %middle_rows.1.middle_ref, f32[1,2048]{1,0:T(1,128)} %bitcast.12), custom_call_target="tpu_custom_call" | custom-call | tf_op jit(solution)/shard_map/closing_rows/pallas_call | solution.py:383
Async XLA Ops:
  6.5 123.1 %all-gather.2.cloned.1.call-start = ((), (), s32[]{:S(2)}) async-start(), calls=%async_computation.6 | async-start | bytes 5308416 | tf_op jit(solution)/shard_map/all_gather | solution.py:426
  42.3 15.7 %all-to-all-start = ((bf16[8,64,512]{2,1,0:T(8,128)(2,1)}), bf16[8,64,512]{2,1,0:T(8,128)(2,1)S(1)}, u32[]{:S(2)}, u32[]{:S(2)}) async-start(bf16[8,64,512]{2,1,0:T(8,128)(2,1)} %get-tuple-element.9), calls=%async_computation | async-start | bytes 1048576 | tf_op jit(solution)/shard_map/all_to_all | solution.py:312
  57.9 0.8 copy-start
Sparse Core Ops, SparseCore 0:
  32.7 72.4 all-gather.1

commit v2 on v1

--- a/solution.py
+++ b/solution.py
@@ -1,4 +1,3 @@
-import functools
 import math
 
 import jax
@@ -243,7 +242,8 @@
 
 def middle_rows(place_ref, got_ref, skip_ref, gain_ref, send_ref):
     summed = jnp.sum(got_ref[...].astype(F32), axis=0)
-    summed = summed + RESIDUAL_SCALE * skip_ref[...].astype(F32)
+    mine = skip_ref[pl.ds(pl.multiple_of(place_ref[2] * 8, 8), 8), :]
+    summed = summed + RESIDUAL_SCALE * mine.astype(F32)
     middle = normed_rows(summed, gain_ref[...]).astype(BF16)
     for peer in range(send_ref.shape[0]):
         send_ref[peer] = middle
@@ -256,16 +256,11 @@
 
 
 def pack_weights(valve_ref, widen_ref, shrink_ref, send_ref):
-    rows = valve_ref.shape[0]
-    eye = (iota((rows, rows), 0) == iota((rows, rows), 1)).astype(BF16)
-    turned = lax.dot_general(
-        eye, shrink_ref[...], (((1,), (1,)), ((), ())), preferred_element_type=F32
-    ).astype(BF16)
-    blank = jnp.zeros((rows, 2 * PART - UNITS), BF16)
+    blank = jnp.zeros((valve_ref.shape[0], 2 * PART - UNITS), BF16)
     halves = []
     for lo in (0, PART):
         line = []
-        for whole in (valve_ref[...], widen_ref[...], turned):
+        for whole in (valve_ref[...], widen_ref[...], shrink_ref[...]):
             line.append(whole[:, lo : lo + PART])
             if lo:
                 line.append(blank)
@@ -305,7 +300,19 @@
 
 
 def shape(dims, kind=BF16):
-    return jax.ShapeDtypeStruct(dims, kind)
+    return pltpu.VMEM(dims, kind)
+
+
+def near(*arrays):
+    return [pltpu.with_memory_space_constraint(a, pltpu.VMEM) for a in arrays]
+
+
+def cost(us):
+    return pl.CostEstimate(flops=int(us * 2.0e8), transcendentals=0, bytes_accessed=0)
+
+
+def whole(array):
+    return pl.BlockSpec(array.shape, lambda *_: (0,) * array.ndim)
 
 
 def exchanged(value, axis):
@@ -315,9 +322,11 @@
 def run_mixer_local(*args):
     return pl.pallas_call(
         mixer_local,
-        in_specs=[VMEM] * 6,
+        grid=(1,),
+        in_specs=[whole(a) for a in args],
         out_specs=[VMEM] * 2,
         out_shape=[shape((8, HEAD, 4 * WIDE)), shape((2, TOK, 2 * WIDE), F32)],
+        cost_estimate=cost(8),
         name="mixer_local",
     )(*args)
 
@@ -328,8 +337,9 @@
         in_specs=[SMEM, VMEM],
         out_specs=[VMEM] * 2,
         out_shape=[shape((8, HEAD, 2 * WIDE)), shape((2, HEAD, 2 * WIDE), F32)],
+        cost_estimate=cost(3),
         name="combine_near",
-    )(place, got)
+    )(place, *near(got))
 
 
 def run_finish_mixer(place, *args):
@@ -338,26 +348,20 @@
         in_specs=[SMEM] + [VMEM] * (len(args)),
         out_specs=VMEM,
         out_shape=shape((8, 8, D)),
+        cost_estimate=cost(4),
         name="finish_mixer",
-    )(place, *args)
+    )(place, *near(*args))
 
 
 def run_middle_rows(place, got, skip, gain, peers):
     return pl.pallas_call(
         middle_rows,
-        grid_spec=pltpu.PrefetchScalarGridSpec(
-            num_scalar_prefetch=1,
-            grid=(1,),
-            in_specs=[
-                pl.BlockSpec((8, 8, D), lambda i, place: (0, 0, 0)),
-                pl.BlockSpec((8, D), lambda i, place: (place[2], 0)),
-                pl.BlockSpec((1, D), lambda i, place: (0, 0)),
-            ],
-            out_specs=pl.BlockSpec((peers, 8, D), lambda i, place: (0, 0, 0)),
-        ),
+        in_specs=[SMEM] + [VMEM] * 3,
+        out_specs=VMEM,
         out_shape=shape((peers, 8, D)),
+        cost_estimate=cost(2),
         name="middle_rows",
-    )(place, got, skip, gain)
+    )(place, *near(got, skip, gain))
 
 
 def run_feed_forward(rows, weights, peers):
@@ -375,23 +379,20 @@
             pltpu.VMEM((peers * 8, 2 * PART), F32),
             pltpu.VMEM((peers * 8, PART), BF16),
         ],
+        cost_estimate=cost(5),
         name="feed_forward",
-    )(rows, weights, weights)
+    )(*near(rows), weights, weights)
 
 
 def run_closing_rows(got, middle, gain):
     return pl.pallas_call(
         closing_rows,
-        grid=(1,),
-        in_specs=[
-            pl.BlockSpec(got.shape, lambda i: (0, 0, 0)),
-            pl.BlockSpec((1, 8, D), lambda i: (0, 0, 0)),
-            pl.BlockSpec((1, D), lambda i: (0, 0)),
-        ],
-        out_specs=pl.BlockSpec((8, D), lambda i: (0, 0)),
-        out_shape=shape((8, D)),
+        in_specs=[VMEM] * 3,
+        out_specs=VMEM,
+        out_shape=jax.ShapeDtypeStruct((8, D), BF16),
+        cost_estimate=cost(2),
         name="closing_rows",
-    )(got, middle, gain)
+    )(*near(got, middle, gain))
 
 
 def shards(
@@ -415,16 +416,17 @@
     place = jnp.stack([lax.axis_index(Y), lax.axis_index("z"), lax.axis_index("tp")]).astype(
         jnp.int32
     )
+    given = (perceptron_valve_factors, perceptron_widen_factors, perceptron_shrink_factors.T)
     packed = pl.pallas_call(
         pack_weights,
-        in_specs=[VMEM] * 3,
+        grid=(1,),
+        in_specs=[whole(a) for a in given],
         out_specs=VMEM,
         out_shape=shape((8, 32, 3 * PART)),
+        cost_estimate=cost(2),
         name="pack_weights",
-    )(perceptron_valve_factors, perceptron_widen_factors, perceptron_shrink_factors)
-    near_weights = exchanged(packed, Y).reshape(256, 3 * PART)
-    weights = lax.all_gather(near_weights, "z", axis=0, tiled=True)
-
+    )(*given)
+    near_weights = exchanged(packed, Y)
     sends, local = run_mixer_local(
         reading_vectors,
         blender_lookup_labels,
@@ -433,6 +435,7 @@
         amend_speed_logits,
         extra_log_fades,
     )
+    weights = lax.all_gather(near_weights.reshape(256, 3 * PART), "z", axis=0, tiled=True)
     totals, before = run_combine_near(place, exchanged(sends, Y))
     shares = run_finish_mixer(
         place,

time: 159 us -> 146 us (0.918)
  Pallas kernels: 30.1 us -> 22.8 us
  blocking collectives: 96.9 us -> 92.1 us
  local copies, waits for them, and re-layouts: 2.43 us -> 0.06 us
    all_to_all x5, blocking collectives: 96.9 us -> 92.1 us  [exchanged(): return lax.all_to_all(value, axis, 0, 0, tiled=True)]
    pallas_call x4, Pallas kernels: 16.4 us -> 12.4 us  [the longest x1 9.73 us: run_mixer_local(): pl.pallas_call(mixer_local, grid=(1,), in_specs=[whole(a) for a in args],...]
    unnamed x3 -> x22, local copies, waits for them, and re-layouts: 2.43 us -> 0.06 us
  transfers between devices with their start and end apart: 2 -> 2, of which waited for: 1 -> 1; matrix products, arithmetic and copies ran while one was open for 0% -> 0% of each run, Pallas kernels for 13% -> 12%
where the time goes in v2:
time: 146 us; the launch traced here: 145 us
  blocking collectives  92.1 us (63%)
  Pallas kernels  22.8 us (16%)
  between operations  13.6 us (9%)
  waiting for transfers between devices  12.3 us (8%)
  starting transfers between devices  3.63 us (2%)
    all_to_all x5, blocking collectives, exchanged(): return lax.all_to_all(value, axis, 0, 0, tiled=True)  92.1 us
    all_to_all x1, waiting for transfers between devices, exchanged(): return lax.all_to_all(value, axis, 0, 0, tiled=True)  12.3 us
    pallas_call x1, Pallas kernels, run_mixer_local(): pl.pallas_call(mixer_local, grid=(1,), in_specs=[whole(a) for a in args],...  9.73 us
    pallas_call x1, Pallas kernels, run_feed_forward(): pl.pallas_call(feed_forward, grid=(2 * STEPS,), in_specs=[pl.BlockSpec((p...  4.18 us
    pallas_call x1, Pallas kernels, run_finish_mixer(): pl.pallas_call(finish_mixer, in_specs=[SMEM] + [VMEM] * len(args), out_sp...  3.68 us
    all_to_all x1, starting transfers between devices, exchanged(): return lax.all_to_all(value, axis, 0, 0, tiled=True)  3.62 us
  transfers between devices with their start and end apart: 2, of which 1 were waited for; matrix products, arithmetic and copies ran while one was open for 0% of the time, Pallas kernels for 12%

profile of v2, /device:TPU:1, one launch (start us, length us, event | category | flops | bytes accessed | tf_op | source)
XLA Modules:
  0.0 145.0 jit_solution(12825851440659597493)
XLA Ops:
  6.5 0.0 all-gather.2.cloned.1.call-start
  6.5 0.9 pack_weights.1
  7.4 23.3 %all_to_all.30 = bf16[8,32,1152]{2,1,0:T(8,128)(2,1)} all-to-all(bf16[8,32,1152]{2,1,0:T(8,128)(2,1)S(1)} %pack_weights.1), channel_id=1, replica_groups=mesh['z'=8,'yh'=4,'yl'=2,'tp'=8] {'yh','yl'}, dimensions={0} | all-to-all | bytes 1179648 | tf_op jit(solution)/shard_map/all_to_all | solution.py:319
  30.7 0.0 all-gather.2.cloned.1.call-update
  30.7 0.0 copy-start
  30.7 0.0 copy-start.2
  30.8 0.0 copy-start.3
  30.8 0.0 copy-start.4
  30.8 0.0 copy-start.5
  30.8 0.0 copy-start.6
  30.8 0.0 copy-start.9
  30.8 0.0 copy-start.10
  30.8 9.7 %mixer_local.1 = (bf16[8,64,512]{2,1,0:T(8,128)(2,1)}, f32[2,64,256]{2,1,0:T(8,128)S(1)}) custom-call(bf16[64,128]{1,0:T(8,128)(2,1)} %reads_ref.3, bf16[64,128]{1,0:T(8,128)(2,1)} %keys_ref.3, bf16[64,128]{1,0:T(8,128)(2,1)} %values_ref.3, bf16[2,64,128]{2,1,0:T(8,128)(2,1)} %fades_ref.1, bf16[2,64,128]{2,1,0:T(8,128)(2,1)} %rates_ref.3, f32[2,2,64]{2,1,0:T(2,128)} %extra_ref.1), custom_call_target="tpu_custom_call" | custom-call | flops 1600000000 | tf_op jit(solution)/shard_map/mixer_local/pallas_call | solution.py:323
  40.6 0.0 copy-start.1
  40.6 0.0 copy-start.7
  40.6 3.6 %all-to-all-start = ((bf16[8,64,512]{2,1,0:T(8,128)(2,1)}), bf16[8,64,512]{2,1,0:T(8,128)(2,1)S(1)}, u32[]{:S(2)}, u32[]{:S(2)}) async-start(bf16[8,64,512]{2,1,0:T(8,128)(2,1)} %get-tuple-element.9), calls=%async_computation | async-start | bytes 1048576 | tf_op jit(solution)/shard_map/all_to_all | solution.py:319
  44.2 0.7 pad_add_fusion.place_ref
  44.9 12.3 %all-to-all-done.got_ref = bf16[8,64,512]{2,1,0:T(8,128)(2,1)S(1)} async-done(((bf16[8,64,512]{2,1,0:T(8,128)(2,1)}), bf16[8,64,512]{2,1,0:T(8,128)(2,1)S(1)}, u32[]{:S(2)}, u32[]{:S(2)}) %all-to-all-start) | async-done | bytes 524320 | tf_op jit(solution)/shard_map/all_to_all | solution.py:319
  57.1 2.5 %combine_near.1 = (bf16[8,64,256]{2,1,0:T(8,128)(2,1)S(1)}, f32[2,64,256]{2,1,0:T(8,128)S(1)}) custom-call(s32[3]{0:T(128)} %pad_add_fusion.place_ref, bf16[8,64,512]{2,1,0:T(8,128)(2,1)S(1)} %all-to-all-done.got_ref), custom_call_target="tpu_custom_call" | custom-call | flops 600000000 | tf_op jit(solution)/shard_map/combine_near/pallas_call | solution.py:335
  59.6 27.8 %all_to_all.31.got_ref = bf16[8,64,256]{2,1,0:T(8,128)(2,1)S(1)} all-to-all(bf16[8,64,256]{2,1,0:T(8,128)(2,1)S(1)} %get-tuple-element.10), channel_id=1, replica_groups=mesh['z'=8,'yh'=4,'yl'=2,'tp'=8] {'z'}, dimensions={0} | all-to-all | bytes 524288 | tf_op jit(solution)/shard_map/all_to_all | solution.py:319
  87.4 0.0 copy-done
  87.4 0.0 copy-done.2
  87.4 0.0 copy-done.3
  87.4 0.0 copy-done.4
  87.4 0.0 copy-done.5
  87.4 0.0 copy-done.6
  87.4 0.0 copy-done.9
  87.4 0.0 copy-done.10
  87.4 3.7 %finish_mixer.1 = bf16[8,8,2048]{2,1,0:T(8,128)(2,1)S(1)} custom-call(s32[3]{0:T(128)} %pad_add_fusion.place_ref, bf16[8,64,256]{2,1,0:T(8,128)(2,1)S(1)} %all_to_all.31.got_ref, f32[2,64,256]{2,1,0:T(8,128)S(1)} %get-tuple-element.11.pre_ref, f32[2,64,256]{2,1,0:T(8,128)S(1)} %get-tuple-element.12.local_ref, bf16[64,128]{1,0:T(8,128)(2,1)S(1)} %copy-done.3, ...), custom_call_target="tpu_custom_call" | custom-call | flops 800000000 | tf_op jit(solution)/shard_map/finish_mixer/pallas_call | solution.py:346
  91.1 14.4 %all_to_all.32.got_ref = bf16[8,8,2048]{2,1,0:T(8,128)(2,1)S(1)} all-to-all(bf16[8,8,2048]{2,1,0:T(8,128)(2,1)S(1)} %finish_mixer.1), channel_id=1, replica_groups=mesh['z'=8,'yh'=4,'yl'=2,'tp'=8] {'tp'}, dimensions={0} | all-to-all | bytes 524288 | tf_op jit(solution)/shard_map/all_to_all | solution.py:319
  105.5 0.0 copy-done.1
  105.5 0.0 copy-done.7
  105.5 0.9 middle_rows.1.middle_ref
  106.4 13.2 %all_to_all.33 = bf16[16,8,2048]{2,1,0:T(8,128)(2,1)S(1)} all-to-all(bf16[16,8,2048]{2,1,0:T(8,128)(2,1)S(1)} %middle_rows.1.middle_ref), channel_id=1, replica_groups=mesh['z'=8,'yh'=4,'yl'=2,'tp'=8] {'yl','tp'}, dimensions={0} | all-to-all | bytes 1048576 | tf_op jit(solution)/shard_map/all_to_all | solution.py:319
  119.7 0.0 all-gather.2.cloned.1.call-done.up_ref.down_ref
  119.7 0.0 copy-start.8
  119.7 4.2 %feed_forward.1 = bf16[16,8,2048]{2,1,0:T(8,128)(2,1)S(1)} custom-call(bf16[128,2048]{1,0:T(8,128)(2,1)S(1)} %bitcast.10, bf16[2048,1152]{1,0:T(8,128)(2,1)} %all-gather.2.cloned.1.call-done.up_ref.down_ref, bf16[2048,1152]{1,0:T(8,128)(2,1)} %all-gather.2.cloned.1.call-done.up_ref.down_ref), custom_call_target="tpu_custom_call" | custom-call | flops 1000000000 | tf_op jit(solution)/shard_map/feed_forward/pallas_call | solution.py:368
  123.8 13.4 %all_to_all.34.got_ref = bf16[16,8,2048]{2,1,0:T(8,128)(2,1)S(1)} all-to-all(bf16[16,8,2048]{2,1,0:T(8,128)(2,1)S(1)} %feed_forward.1), channel_id=1, replica_groups=mesh['z'=8,'yh'=4,'yl'=2,'tp'=8] {'yl','tp'}, dimensions={0} | all-to-all | bytes 1048576 | tf_op jit(solution)/shard_map/all_to_all | solution.py:319
  137.3 0.0 copy-done.8
  137.3 0.9 closing_rows.1
Async XLA Ops:
  6.5 113.1 %all-gather.2.cloned.1.call-start = ((), (), s32[]{:S(2)}) async-start(), calls=%async_computation.6 | async-start | bytes 5308416 | tf_op jit(solution)/shard_map/all_gather | solution.py:438
  30.7 56.7 %copy-start = (bf16[128,2048]{1,0:T(8,128)(2,1)S(1)}, bf16[128,2048]{1,0:T(8,128)(2,1)}, u32[]{:S(2)}) copy-start(bf16[128,2048]{1,0:T(8,128)(2,1)} %projector_ref.1) | copy-start | bytes 1572868
  30.7 56.6 %copy-start.2 = (bf16[2,64,128]{2,1,0:T(8,128)(2,1)S(1)}, bf16[2,64,128]{2,1,0:T(8,128)(2,1)}, u32[]{:S(2)}) copy-start(bf16[2,64,128]{2,1,0:T(8,128)(2,1)} %rates_ref.3) | copy-start | bytes 98308
  30.8 56.6 %copy-start.3 = (bf16[64,128]{1,0:T(8,128)(2,1)S(1)}, bf16[64,128]{1,0:T(8,128)(2,1)}, u32[]{:S(2)}) copy-start(bf16[64,128]{1,0:T(8,128)(2,1)} %reads_ref.3) | copy-start | bytes 49156
  30.8 56.6 %copy-start.4 = (bf16[64,128]{1,0:T(8,128)(2,1)S(1)}, bf16[64,128]{1,0:T(8,128)(2,1)}, u32[]{:S(2)}) copy-start(bf16[64,128]{1,0:T(8,128)(2,1)} %keys_ref.3) | copy-start | bytes 49156
  30.8 56.6 %copy-start.5 = (bf16[64,128]{1,0:T(8,128)(2,1)S(1)}, bf16[64,128]{1,0:T(8,128)(2,1)}, u32[]{:S(2)}) copy-start(bf16[64,128]{1,0:T(8,128)(2,1)} %values_ref.3) | copy-start | bytes 49156
  30.8 56.6 %copy-start.6 = (bf16[64,128]{1,0:T(8,128)(2,1)S(1)}, bf16[64,128]{1,0:T(8,128)(2,1)}, u32[]{:S(2)}) copy-start(bf16[64,128]{1,0:T(8,128)(2,1)} %valve_ref.2) | copy-start | bytes 49156
  30.8 56.6 %copy-start.9 = (f32[128]{0:T(128)S(1)}, f32[128]{0:T(128)}, u32[]{:S(2)}) copy-start(f32[128]{0:T(128)} %param.24) | copy-start | bytes 1540
  30.8 56.6 %copy-start.10 = (f32[128]{0:T(128)S(1)}, f32[128]{0:T(128)}, u32[]{:S(2)}) copy-start(f32[128]{0:T(128)} %param.25) | copy-start | bytes 1540
  40.6 64.9 %copy-start.1 = (bf16[64,2048]{1,0:T(8,128)(2,1)S(1)}, bf16[64,2048]{1,0:T(8,128)(2,1)}, u32[]{:S(2)}) copy-start(bf16[64,2048]{1,0:T(8,128)(2,1)} %skip_ref.1) | copy-start | bytes 786436
  40.6 64.9 %copy-start.7 = (f32[2048]{0:T(1024)S(1)}, f32[2048]{0:T(1024)}, u32[]{:S(2)}) copy-start(f32[2048]{0:T(1024)} %param.27) | copy-start | bytes 24580
  40.6 16.6 %all-to-all-start = ((bf16[8,64,512]{2,1,0:T(8,128)(2,1)}), bf16[8,64,512]{2,1,0:T(8,128)(2,1)S(1)}, u32[]{:S(2)}, u32[]{:S(2)}) async-start(bf16[8,64,512]{2,1,0:T(8,128)(2,1)} %get-tuple-element.9), calls=%async_computation | async-start | bytes 1048576 | tf_op jit(solution)/shard_map/all_to_all | solution.py:319
  119.7 17.6 %copy-start.8 = (f32[2048]{0:T(1024)S(1)}, f32[2048]{0:T(1024)}, u32[]{:S(2)}) copy-start(f32[2048]{0:T(1024)} %param.31) | copy-start | bytes 24580
Sparse Core Ops, SparseCore 0:
  30.9 71.3 all-gather.1

commit v3 on v2

--- a/solution.py
+++ b/solution.py
@@ -10,7 +10,7 @@
 
 Y = ("yh", "yl")
 SP = ("z", "yh", "yl")
-SP_TP = ("z", "yh", "yl", "tp")
+SP_TP = SP + ("tp",)
 PEERS = ("yl", "tp")
 
 RESIDUAL_SCALE = 2.0**0.25
@@ -23,6 +23,7 @@
 SUB = 16
 UNITS = 704
 PART = 384
+PEER_COUNT = 16
 D = 2048
 F32 = jnp.float32
 BF16 = jnp.bfloat16
@@ -32,19 +33,47 @@
     return lax.broadcasted_iota(jnp.int32, shape, dim)
 
 
+def split(x):
+    high = x.astype(BF16)
+    return high, (x - high.astype(F32)).astype(BF16)
+
+
+def product(a, b, dims):
+    (a_high, a_low), (b_high, b_low) = split(a), split(b)
+
+    def part(one, two):
+        return lax.dot_general(one, two, (dims, ((), ())), preferred_element_type=F32)
+
+    return part(a_high, b_high) + (part(a_high, b_low) + part(a_low, b_high))
+
+
 def dot(a, b):
-    return jnp.dot(a, b, preferred_element_type=F32, precision=lax.Precision.HIGHEST)
+    return product(a, b, ((1,), (0,)))
 
 
 def dot_nt(a, b):
-    return lax.dot_general(
-        a, b, (((1,), (1,)), ((), ())), preferred_element_type=F32, precision=lax.Precision.HIGHEST
-    )
+    return product(a, b, ((1,), (1,)))
 
 
 def dot_tn(a, b):
-    return lax.dot_general(
-        a, b, (((0,), (0,)), ((), ())), preferred_element_type=F32, precision=lax.Precision.HIGHEST
+    return product(a, b, ((0,), (0,)))
+
+
+def chosen(picks, x, dims=((1,), (0,))):
+    high, middle = split(x)
+    low = (x - high.astype(F32) - middle.astype(F32)).astype(BF16)
+    parts = [
+        lax.dot_general(picks, part, (dims, ((), ())), preferred_element_type=F32)
+        for part in (high, middle, low)
+    ]
+    return parts[0] + (parts[1] + parts[2])
+
+
+def head_sums(x):
+    high, low = split(x)
+    ones = head_ones().astype(BF16)
+    return jnp.dot(high, ones, preferred_element_type=F32) + jnp.dot(
+        low, ones, preferred_element_type=F32
     )
 
 
@@ -71,6 +100,17 @@
 
 def sigmoid(x):
     return 1.0 / (1.0 + jnp.exp(-x))
+
+
+def spread_heads(extra):
+    lanes_of = (iota((2, WIDE), 1) // HEAD == iota((2, WIDE), 0)).astype(BF16)
+    high, middle = split(extra)
+    low = (extra - high.astype(F32) - middle.astype(F32)).astype(BF16)
+    parts = [
+        lax.dot_general(part, lanes_of, (((0,), (0,)), ((), ())), preferred_element_type=F32)
+        for part in (high, middle, low)
+    ]
+    return parts[0] + (parts[1] + parts[2])
 
 
 def unit_lower_inverse(a):
@@ -91,7 +131,7 @@
     refill, write = unit * rate, keys * rate
     row, col = iota((TOK, TOK), 0), iota((TOK, TOK), 1)
     reach = (col >= row) if back else (col <= row)
-    upto = dot(reach.astype(F32), log_decay)
+    upto = chosen(reach.astype(BF16), log_decay)
     ahead = upto - log_decay
     whole = upto[:1] if back else upto[TOK - 1 :]
     low = low_half((SUB, WIDE))
@@ -153,12 +193,10 @@
 def mixer_local(reads_ref, keys_ref, values_ref, fades_ref, rates_ref, extra_ref, send_ref, out_ref):
     reads, keys = reads_ref[...].astype(F32), keys_ref[...].astype(F32)
     values = values_ref[...].astype(F32)
-    unit = keys * lax.rsqrt(dot(keys * keys, head_ones()) + KEY_EPS)
-    lanes_of = (iota((2, WIDE), 1) // HEAD == iota((2, WIDE), 0)).astype(F32)
+    unit = keys * lax.rsqrt(head_sums(keys * keys) + KEY_EPS)
     for way in range(2):
-        log_decay = -math.exp(-0.5) * sigmoid(fades_ref[way].astype(F32)) + dot_tn(
-            extra_ref[way], lanes_of
-        )
+        log_decay = -math.exp(-0.5) * sigmoid(fades_ref[way].astype(F32))
+        log_decay = log_decay + spread_heads(extra_ref[way])
         rate = sigmoid(rates_ref[way].astype(F32))
         out, state = one_way(way == 1, reads, unit, keys, values, log_decay, rate)
         out_ref[way] = out
@@ -168,7 +206,13 @@
 
 
 def advanced(piece, running):
-    moved = dot(piece[:, WIDE:], by_head(running))
+    high, low = split(by_head(running))
+    step = piece[:, WIDE:]
+    if step.dtype == F32:
+        moved = dot(step, by_head(running))
+    else:
+        moved = jnp.dot(step, high, preferred_element_type=F32)
+        moved = moved + jnp.dot(step, low, preferred_element_type=F32)
     if running.shape[1] == WIDE:
         return moved + piece[:, :WIDE]
     return moved + jnp.concatenate([piece[:, :WIDE], jnp.zeros((HEAD, WIDE), F32)], axis=1)
@@ -181,7 +225,7 @@
     for step in range(8):
         for way in range(2):
             k = 7 - step if way else step
-            piece = got_ref[k, :, way * 2 * WIDE : (way + 1) * 2 * WIDE].astype(F32)
+            piece = got_ref[k, :, way * 2 * WIDE : (way + 1) * 2 * WIDE]
             total[way] = advanced(piece, total[way])
             passed = (k > y) if way else (k < y)
             before[way] = jnp.where(passed, total[way], before[way])
@@ -214,20 +258,19 @@
             k = 7 - step if way else step
             passed = (k > z) if way else (k < z)
             state[way] = jnp.where(
-                passed, advanced(got_ref[k].astype(F32), state[way]), state[way]
+                passed, advanced(got_ref[k], state[way]), state[way]
             )
     summed = 0.0
     for way in range(2):
         entering = advanced(pre_ref[way], state[way])
         summed = summed + local_ref[way, :, :WIDE]
         summed = summed + dot(local_ref[way, :, WIDE:], by_head(entering))
-    ones = head_ones()
-    off = summed - dot(summed, ones) * (1.0 / HEAD)
-    spread = dot(off * off, ones) * (1.0 / HEAD)
+    off = summed - head_sums(summed) * (1.0 / HEAD)
+    spread = head_sums(off * off) * (1.0 / HEAD)
     normed = off * lax.rsqrt(spread + GROUP_EPS) * gain_ref[...]
     keys = keys_ref[...].astype(F32)
     both = keys * sigmoid(rates_ref[0].astype(F32)) + keys * sigmoid(rates_ref[1].astype(F32))
-    bonus = dot(reads_ref[...].astype(F32) * both * reward_ref[...], ones)
+    bonus = head_sums(reads_ref[...].astype(F32) * both * reward_ref[...])
     bonus = bonus * values_ref[...].astype(F32)
     mixed = ((normed + bonus) * valve_ref[...].astype(F32)).astype(BF16)
     share = jnp.dot(mixed, projector_ref[...], preferred_element_type=F32)
@@ -269,30 +312,33 @@
         send_ref[peer] = halves[peer % 2]
 
 
-CHUNK = 1024
-STEPS = D // CHUNK
-
-
-def feed_forward(rows_ref, up_ref, down_ref, out_ref, acc_ref, inner_ref):
-    step = pl.program_id(0)
-
-    @pl.when(step < STEPS)
-    def _():
-        at = pl.multiple_of(step * CHUNK, CHUNK)
-        part = jnp.dot(rows_ref[:, pl.ds(at, CHUNK)], up_ref[...], preferred_element_type=F32)
-        acc_ref[...] = jnp.where(step == 0, part, acc_ref[...] + part)
-
-    @pl.when(step == STEPS - 1)
-    def _():
-        gate, up = acc_ref[:, :PART], acc_ref[:, PART:]
-        inner_ref[...] = (gate / (1.0 + jnp.exp(-gate)) * up).astype(BF16)
-
-    @pl.when(step >= STEPS)
-    def _():
+PLANE = 256
+PARTS = D // PLANE
+
+
+def feed_forward(rows_ref, weights_ref, out_ref, held_ref, arrived):
+    copies = []
+    for k in range(PARTS):
+        rows = pl.ds(k * PLANE, PLANE)
+        copies.append(
+            pltpu.make_async_copy(weights_ref.at[rows], held_ref.at[rows], arrived.at[k])
+        )
+        copies[k].start()
+    sums = 0.0
+    for k in range(PARTS):
+        copies[k].wait()
+        rows = slice(k * PLANE, (k + 1) * PLANE)
+        sums = sums + jnp.dot(
+            rows_ref[:, rows], held_ref[rows, : 2 * PART], preferred_element_type=F32
+        )
+    gate, up = sums[:, :PART], sums[:, PART:]
+    inner = (gate / (1.0 + jnp.exp(-gate)) * up).astype(BF16)
+    for k in range(PARTS):
+        rows = slice(k * PLANE, (k + 1) * PLANE)
         share = lax.dot_general(
-            inner_ref[...], down_ref[...], (((1,), (1,)), ((), ())), preferred_element_type=F32
+            inner, held_ref[rows, 2 * PART :], (((1,), (1,)), ((), ())), preferred_element_type=F32
         )
-        out_ref[...] = share.astype(BF16).reshape(out_ref.shape)
+        out_ref[:, :, rows] = share.astype(BF16).reshape(PEER_COUNT, 8, PLANE)
 
 
 VMEM = pl.BlockSpec(memory_space=pltpu.VMEM)
@@ -364,24 +410,19 @@
     )(place, *near(got, skip, gain))
 
 
-def run_feed_forward(rows, weights, peers):
+def run_feed_forward(rows, weights):
     return pl.pallas_call(
         feed_forward,
-        grid=(2 * STEPS,),
-        in_specs=[
-            pl.BlockSpec((peers * 8, D), lambda i: (0, 0)),
-            pl.BlockSpec((CHUNK, 2 * PART), lambda i: (jnp.minimum(i, STEPS - 1), 0)),
-            pl.BlockSpec((CHUNK, PART), lambda i: (jnp.maximum(i - STEPS, 0), 2)),
+        in_specs=[VMEM, pl.BlockSpec(memory_space=pl.ANY)],
+        out_specs=VMEM,
+        out_shape=shape((PEER_COUNT, 8, D)),
+        scratch_shapes=[
+            pltpu.VMEM((D, 3 * PART), BF16),
+            pltpu.SemaphoreType.DMA((PARTS,)),
         ],
-        out_specs=pl.BlockSpec((peers, 8, CHUNK), lambda i: (0, 0, jnp.maximum(i - STEPS, 0))),
-        out_shape=shape((peers, 8, D)),
-        scratch_shapes=[
-            pltpu.VMEM((peers * 8, 2 * PART), F32),
-            pltpu.VMEM((peers * 8, PART), BF16),
-        ],
-        cost_estimate=cost(5),
+        cost_estimate=cost(4),
         name="feed_forward",
-    )(*near(rows), weights, weights)
+    )(*near(rows), weights)
 
 
 def run_closing_rows(got, middle, gain):
@@ -426,7 +467,7 @@
         cost_estimate=cost(2),
         name="pack_weights",
     )(*given)
-    near_weights = exchanged(packed, Y)
+    own = exchanged(packed, Y).reshape(PLANE, 3 * PART)
     sends, local = run_mixer_local(
         reading_vectors,
         blender_lookup_labels,
@@ -435,11 +476,13 @@
         amend_speed_logits,
         extra_log_fades,
     )
-    weights = lax.all_gather(near_weights.reshape(256, 3 * PART), "z", axis=0, tiled=True)
-    totals, before = run_combine_near(place, exchanged(sends, Y))
+    near_states = exchanged(sends, Y)
+    weights = [lax.all_gather(own, "z", axis=0, tiled=True)]
+    totals, before = run_combine_near(place, near_states)
+    far_states = exchanged(totals, "z")
     shares = run_finish_mixer(
         place,
-        exchanged(totals, "z"),
+        far_states,
         before,
         local,
         reading_vectors,
@@ -451,13 +494,14 @@
         attender_scaling_vector.reshape(1, WIDE),
         blender_result_projector,
     )
-    peers = 16
+    shares = exchanged(shares, "tp")
     middle = run_middle_rows(
-        place, exchanged(shares, "tp"), skip_stream_entering, blender_scaling_vector.reshape(1, D), peers
-    )
-    rows = exchanged(middle, PEERS).reshape(peers * 8, D)
-    down = run_feed_forward(rows, weights, peers)
-    return run_closing_rows(exchanged(down, PEERS), middle, closing_scaling_vector.reshape(1, D))
+        place, shares, skip_stream_entering, blender_scaling_vector.reshape(1, D), PEER_COUNT
+    )
+    rows = exchanged(middle, PEERS).reshape(PEER_COUNT * 8, D)
+    down = run_feed_forward(rows, weights[0])
+    down = exchanged(down, PEERS)
+    return run_closing_rows(down, middle, closing_scaling_vector.reshape(1, D))
 
 
 def solution(mesh):

time: 146 us -> 141 us (0.966)
  Pallas kernels: 22.8 us -> 18.4 us
    pallas_call x1, Pallas kernels: 9.73 us -> 7.3 us  [run_mixer_local(): pl.pallas_call(mixer_local, grid=(1,), in_specs=[whole(a) for a in args],...]
  transfers between devices with their start and end apart: 2 -> 2, of which waited for: 1 -> 1; matrix products, arithmetic and copies ran while one was open for 0% -> 0% of each run, Pallas kernels for 12% -> 10%
where the time goes in v3:
time: 141 us
  blocking collectives  92 us (65%)
  Pallas kernels  18.4 us (13%)
  between operations  13.6 us (10%)
  waiting for transfers between devices  12.3 us (9%)
  starting transfers between devices  3.63 us (3%)
    all_to_all x5, blocking collectives, exchanged(): return lax.all_to_all(value, axis, 0, 0, tiled=True)  92 us
    all_to_all x1, waiting for transfers between devices, exchanged(): return lax.all_to_all(value, axis, 0, 0, tiled=True)  12.3 us
    pallas_call x1, Pallas kernels, run_mixer_local(): pl.pallas_call(mixer_local, grid=(1,), in_specs=[whole(a) for a in args],...  7.3 us
    all_to_all x1, starting transfers between devices, exchanged(): return lax.all_to_all(value, axis, 0, 0, tiled=True)  3.62 us
    pallas_call x1, Pallas kernels, run_feed_forward(): pl.pallas_call(feed_forward, in_specs=[VMEM, pl.BlockSpec(memory_space=pl...  3.23 us
    pallas_call x1, Pallas kernels, run_finish_mixer(): pl.pallas_call(finish_mixer, in_specs=[SMEM] + [VMEM] * len(args), out_sp...  2.89 us
  transfers between devices with their start and end apart: 2, of which 1 were waited for; matrix products, arithmetic and copies ran while one was open for 0% of the time, Pallas kernels for 10%

profile of v3, /device:TPU:1, one launch (start us, length us, event | category | flops | bytes accessed | tf_op | source)
XLA Modules:
  0.0 140.7 jit_solution(12684871307826096569)
XLA Ops:
  6.5 0.0 all-gather.2.cloned.1.call-start
  6.5 0.9 pack_weights.1
  7.4 23.3 %all_to_all.30 = bf16[8,32,1152]{2,1,0:T(8,128)(2,1)} all-to-all(bf16[8,32,1152]{2,1,0:T(8,128)(2,1)S(1)} %pack_weights.1), channel_id=1, replica_groups=mesh['z'=8,'yh'=4,'yl'=2,'tp'=8] {'yh','yl'}, dimensions={0} | all-to-all | bytes 1179648 | tf_op jit(solution)/shard_map/all_to_all | solution.py:365
  30.7 0.0 all-gather.2.cloned.1.call-update
  30.7 0.0 copy-start
  30.7 0.0 copy-start.2
  30.8 0.0 copy-start.3
  30.8 0.0 copy-start.4
  30.8 0.0 copy-start.5
  30.8 0.0 copy-start.6
  30.8 0.0 copy-start.9
  30.8 0.0 copy-start.10
  30.8 7.3 %mixer_local.1 = (bf16[8,64,512]{2,1,0:T(8,128)(2,1)}, f32[2,64,256]{2,1,0:T(8,128)S(1)}) custom-call(bf16[64,128]{1,0:T(8,128)(2,1)} %reads_ref.3, bf16[64,128]{1,0:T(8,128)(2,1)} %keys_ref.3, bf16[64,128]{1,0:T(8,128)(2,1)} %values_ref.3, bf16[2,64,128]{2,1,0:T(8,128)(2,1)} %fades_ref.1, bf16[2,64,128]{2,1,0:T(8,128)(2,1)} %rates_ref.3, f32[2,2,64]{2,1,0:T(2,128)} %extra_ref.1), custom_call_target="tpu_custom_call" | custom-call | flops 1600000000 | tf_op jit(solution)/shard_map/mixer_local/pallas_call | solution.py:369
  38.1 0.0 copy-start.1
  38.1 0.0 copy-start.7
  38.1 3.6 %all-to-all-start = ((bf16[8,64,512]{2,1,0:T(8,128)(2,1)}), bf16[8,64,512]{2,1,0:T(8,128)(2,1)S(1)}, u32[]{:S(2)}, u32[]{:S(2)}) async-start(bf16[8,64,512]{2,1,0:T(8,128)(2,1)} %get-tuple-element.9), calls=%async_computation | async-start | bytes 1048576 | tf_op jit(solution)/shard_map/all_to_all | solution.py:365
  41.8 0.7 pad_add_fusion.place_ref
  42.4 12.3 %all-to-all-done.got_ref = bf16[8,64,512]{2,1,0:T(8,128)(2,1)S(1)} async-done(((bf16[8,64,512]{2,1,0:T(8,128)(2,1)}), bf16[8,64,512]{2,1,0:T(8,128)(2,1)S(1)}, u32[]{:S(2)}, u32[]{:S(2)}) %all-to-all-start) | async-done | bytes 524320 | tf_op jit(solution)/shard_map/all_to_all | solution.py:365
  54.7 2.2 %combine_near.1 = (bf16[8,64,256]{2,1,0:T(8,128)(2,1)S(1)}, f32[2,64,256]{2,1,0:T(8,128)S(1)}) custom-call(s32[3]{0:T(128)} %pad_add_fusion.place_ref, bf16[8,64,512]{2,1,0:T(8,128)(2,1)S(1)} %all-to-all-done.got_ref), custom_call_target="tpu_custom_call" | custom-call | flops 600000000 | tf_op jit(solution)/shard_map/combine_near/pallas_call | solution.py:381
  56.9 27.8 %all_to_all.31.got_ref = bf16[8,64,256]{2,1,0:T(8,128)(2,1)S(1)} all-to-all(bf16[8,64,256]{2,1,0:T(8,128)(2,1)S(1)} %get-tuple-element.10), channel_id=1, replica_groups=mesh['z'=8,'yh'=4,'yl'=2,'tp'=8] {'z'}, dimensions={0} | all-to-all | bytes 524288 | tf_op jit(solution)/shard_map/all_to_all | solution.py:365
  84.7 0.0 copy-done
  84.7 0.0 copy-done.2
  84.7 0.0 copy-done.3
  84.7 0.0 copy-done.4
  84.7 0.0 copy-done.5
  84.7 0.0 copy-done.6
  84.7 0.0 copy-done.9
  84.7 0.0 copy-done.10
  84.8 2.9 %finish_mixer.1 = bf16[8,8,2048]{2,1,0:T(8,128)(2,1)S(1)} custom-call(s32[3]{0:T(128)} %pad_add_fusion.place_ref, bf16[8,64,256]{2,1,0:T(8,128)(2,1)S(1)} %all_to_all.31.got_ref, f32[2,64,256]{2,1,0:T(8,128)S(1)} %get-tuple-element.11.pre_ref, f32[2,64,256]{2,1,0:T(8,128)S(1)} %get-tuple-element.12.local_ref, bf16[64,128]{1,0:T(8,128)(2,1)S(1)} %copy-done.3, ...), custom_call_target="tpu_custom_call" | custom-call | flops 800000000 | tf_op jit(solution)/shard_map/finish_mixer/pallas_call | solution.py:392
  87.6 14.4 %all_to_all.32.got_ref = bf16[8,8,2048]{2,1,0:T(8,128)(2,1)S(1)} all-to-all(bf16[8,8,2048]{2,1,0:T(8,128)(2,1)S(1)} %finish_mixer.1), channel_id=1, replica_groups=mesh['z'=8,'yh'=4,'yl'=2,'tp'=8] {'tp'}, dimensions={0} | all-to-all | bytes 524288 | tf_op jit(solution)/shard_map/all_to_all | solution.py:365
  102.0 0.0 copy-start.8
  102.0 0.0 copy-done.1
  102.0 0.0 copy-done.7
  102.0 1.1 middle_rows.1.middle_ref
  103.1 13.2 %all_to_all.33 = bf16[16,8,2048]{2,1,0:T(8,128)(2,1)S(1)} all-to-all(bf16[16,8,2048]{2,1,0:T(8,128)(2,1)S(1)} %middle_rows.1.middle_ref), channel_id=1, replica_groups=mesh['z'=8,'yh'=4,'yl'=2,'tp'=8] {'yl','tp'}, dimensions={0} | all-to-all | bytes 1048576 | tf_op jit(solution)/shard_map/all_to_all | solution.py:365
  116.3 0.0 all-gather.2.cloned.1.call-done.weights_ref
  116.3 3.2 %feed_forward.1 = bf16[16,8,2048]{2,1,0:T(8,128)(2,1)S(1)} custom-call(bf16[128,2048]{1,0:T(8,128)(2,1)S(1)} %bitcast.10, bf16[2048,1152]{1,0:T(8,128)(2,1)} %all-gather.2.cloned.1.call-done.weights_ref), custom_call_target="tpu_custom_call" | custom-call | flops 800000000 | tf_op jit(solution)/shard_map/feed_forward/pallas_call | solution.py:414
  119.5 13.5 %all_to_all.34.got_ref = bf16[16,8,2048]{2,1,0:T(8,128)(2,1)S(1)} all-to-all(bf16[16,8,2048]{2,1,0:T(8,128)(2,1)S(1)} %feed_forward.1), channel_id=1, replica_groups=mesh['z'=8,'yh'=4,'yl'=2,'tp'=8] {'yl','tp'}, dimensions={0} | all-to-all | bytes 1048576 | tf_op jit(solution)/shard_map/all_to_all | solution.py:365
  132.9 0.0 copy-done.8
  132.9 0.9 closing_rows.1
Async XLA Ops:
  6.5 109.7 %all-gather.2.cloned.1.call-start = ((), (), s32[]{:S(2)}) async-start(), calls=%async_computation.6 | async-start | bytes 5308416 | tf_op jit(solution)/shard_map/all_gather | solution.py:480
  30.7 54.0 %copy-start = (bf16[128,2048]{1,0:T(8,128)(2,1)S(1)}, bf16[128,2048]{1,0:T(8,128)(2,1)}, u32[]{:S(2)}) copy-start(bf16[128,2048]{1,0:T(8,128)(2,1)} %projector_ref.1) | copy-start | bytes 1572868
  30.7 54.0 %copy-start.2 = (bf16[2,64,128]{2,1,0:T(8,128)(2,1)S(1)}, bf16[2,64,128]{2,1,0:T(8,128)(2,1)}, u32[]{:S(2)}) copy-start(bf16[2,64,128]{2,1,0:T(8,128)(2,1)} %rates_ref.3) | copy-start | bytes 98308
  30.8 53.9 %copy-start.3 = (bf16[64,128]{1,0:T(8,128)(2,1)S(1)}, bf16[64,128]{1,0:T(8,128)(2,1)}, u32[]{:S(2)}) copy-start(bf16[64,128]{1,0:T(8,128)(2,1)} %reads_ref.3) | copy-start | bytes 49156
  30.8 53.9 %copy-start.4 = (bf16[64,128]{1,0:T(8,128)(2,1)S(1)}, bf16[64,128]{1,0:T(8,128)(2,1)}, u32[]{:S(2)}) copy-start(bf16[64,128]{1,0:T(8,128)(2,1)} %keys_ref.3) | copy-start | bytes 49156
  30.8 53.9 %copy-start.5 = (bf16[64,128]{1,0:T(8,128)(2,1)S(1)}, bf16[64,128]{1,0:T(8,128)(2,1)}, u32[]{:S(2)}) copy-start(bf16[64,128]{1,0:T(8,128)(2,1)} %values_ref.3) | copy-start | bytes 49156
  30.8 53.9 %copy-start.6 = (bf16[64,128]{1,0:T(8,128)(2,1)S(1)}, bf16[64,128]{1,0:T(8,128)(2,1)}, u32[]{:S(2)}) copy-start(bf16[64,128]{1,0:T(8,128)(2,1)} %valve_ref.2) | copy-start | bytes 49156
  30.8 53.9 %copy-start.9 = (f32[128]{0:T(128)S(1)}, f32[128]{0:T(128)}, u32[]{:S(2)}) copy-start(f32[128]{0:T(128)} %param.24) | copy-start | bytes 1540
  30.8 53.9 %copy-start.10 = (f32[128]{0:T(128)S(1)}, f32[128]{0:T(128)}, u32[]{:S(2)}) copy-start(f32[128]{0:T(128)} %param.25) | copy-start | bytes 1540
  38.1 63.9 %copy-start.1 = (bf16[64,2048]{1,0:T(8,128)(2,1)S(1)}, bf16[64,2048]{1,0:T(8,128)(2,1)}, u32[]{:S(2)}) copy-start(bf16[64,2048]{1,0:T(8,128)(2,1)} %skip_ref.1) | copy-start | bytes 786436
  38.1 63.9 %copy-start.7 = (f32[2048]{0:T(1024)S(1)}, f32[2048]{0:T(1024)}, u32[]{:S(2)}) copy-start(f32[2048]{0:T(1024)} %param.27) | copy-start | bytes 24580
  38.1 16.6 %all-to-all-start = ((bf16[8,64,512]{2,1,0:T(8,128)(2,1)}), bf16[8,64,512]{2,1,0:T(8,128)(2,1)S(1)}, u32[]{:S(2)}, u32[]{:S(2)}) async-start(bf16[8,64,512]{2,1,0:T(8,128)(2,1)} %get-tuple-element.9), calls=%async_computation | async-start | bytes 1048576 | tf_op jit(solution)/shard_map/all_to_all | solution.py:365
  102.0 30.9 %copy-start.8 = (f32[2048]{0:T(1024)S(1)}, f32[2048]{0:T(1024)}, u32[]{:S(2)}) copy-start(f32[2048]{0:T(1024)} %param.31) | copy-start | bytes 24580
Sparse Core Ops, SparseCore 0:
  30.9 71.3 all-gather.1

commit v4 on v3

--- a/solution.py
+++ b/solution.py
@@ -190,7 +190,7 @@
     return joined_heads(out), state
 
 
-def mixer_local(reads_ref, keys_ref, values_ref, fades_ref, rates_ref, extra_ref, send_ref, out_ref):
+def mixer_local(place_ref, reads_ref, keys_ref, values_ref, fades_ref, rates_ref, extra_ref, send_ref, out_ref):
     reads, keys = reads_ref[...].astype(F32), keys_ref[...].astype(F32)
     values = values_ref[...].astype(F32)
     unit = keys * lax.rsqrt(head_sums(keys * keys) + KEY_EPS)
@@ -226,7 +226,7 @@
         for way in range(2):
             k = 7 - step if way else step
             piece = got_ref[k, :, way * 2 * WIDE : (way + 1) * 2 * WIDE]
-            total[way] = advanced(piece, total[way])
+            total[way] = advanced(piece, total[way]) if step else piece.astype(F32)
             passed = (k > y) if way else (k < y)
             before[way] = jnp.where(passed, total[way], before[way])
     for way in range(2):
@@ -253,13 +253,13 @@
 ):
     z = place_ref[1]
     state = [jnp.zeros((HEAD, WIDE), F32)] * 2
-    for step in range(8):
+    for step in range(7):
         for way in range(2):
             k = 7 - step if way else step
             passed = (k > z) if way else (k < z)
-            state[way] = jnp.where(
-                passed, advanced(got_ref[k], state[way]), state[way]
-            )
+            piece = got_ref[k]
+            later = advanced(piece, state[way]) if step else piece[:, :WIDE].astype(F32)
+            state[way] = jnp.where(passed, later, state[way])
     summed = 0.0
     for way in range(2):
         entering = advanced(pre_ref[way], state[way])
@@ -365,16 +365,16 @@
     return lax.all_to_all(value, axis, 0, 0, tiled=True)
 
 
-def run_mixer_local(*args):
+def run_mixer_local(place, *args):
     return pl.pallas_call(
         mixer_local,
         grid=(1,),
-        in_specs=[whole(a) for a in args],
+        in_specs=[SMEM] + [whole(a) for a in args],
         out_specs=[VMEM] * 2,
         out_shape=[shape((8, HEAD, 4 * WIDE)), shape((2, TOK, 2 * WIDE), F32)],
         cost_estimate=cost(8),
         name="mixer_local",
-    )(*args)
+    )(place, *args)
 
 
 def run_combine_near(place, got):
@@ -469,6 +469,7 @@
     )(*given)
     own = exchanged(packed, Y).reshape(PLANE, 3 * PART)
     sends, local = run_mixer_local(
+        place,
         reading_vectors,
         blender_lookup_labels,
         blender_payloads,

time: 141 us -> 139 us (0.986)
  blocking collectives: 92 us -> 108 us
  waiting for transfers between devices: 12.3 us -> 0.02 us
  starting transfers between devices: 3.63 us -> 0.01 us
    all_to_all x5 -> x6, blocking collectives: 92 us -> 108 us  [exchanged(): return lax.all_to_all(value, axis, 0, 0, tiled=True)]
    all_to_all x1 -> x0, waiting for transfers between devices: 12.3 us -> none  [exchanged(): return lax.all_to_all(value, axis, 0, 0, tiled=True)]
    all_to_all x1 -> x0, starting transfers between devices: 3.62 us -> none  [exchanged(): return lax.all_to_all(value, axis, 0, 0, tiled=True)]
  transfers between devices with their start and end apart: 2 -> 1, of which waited for: 1 -> 0; matrix products, arithmetic and copies ran while one was open for 0% -> 0% of each run, Pallas kernels for 10% -> 9%
where the time goes in v4:
time: 139 us
  blocking collectives  108 us (78%)
  Pallas kernels  17.1 us (12%)
  between operations  13.5 us (10%)
    all_to_all x6, blocking collectives, exchanged(): return lax.all_to_all(value, axis, 0, 0, tiled=True)  108 us
    pallas_call x1, Pallas kernels, run_mixer_local(): pl.pallas_call(mixer_local, grid=(1,), in_specs=[SMEM] + [whole(a) for a...  6.49 us
    pallas_call x1, Pallas kernels, run_feed_forward(): pl.pallas_call(feed_forward, in_specs=[VMEM, pl.BlockSpec(memory_space=pl...  3.22 us
  transfers between devices with their start and end apart: 1, of which 0 were waited for; matrix products, arithmetic and copies ran while one was open for 0% of the time, Pallas kernels for 9%

profile of v4, /device:TPU:1, one launch (start us, length us, event | category | flops | bytes accessed | tf_op | source)
XLA Modules:
  0.0 139.0 jit_solution(13412331856360543071)
XLA Ops:
  6.5 0.0 all-gather.2.cloned.1.call-start
  6.5 0.9 pack_weights.1
  7.4 23.3 %all_to_all.30 = bf16[8,32,1152]{2,1,0:T(8,128)(2,1)} all-to-all(bf16[8,32,1152]{2,1,0:T(8,128)(2,1)S(1)} %pack_weights.1), channel_id=1, replica_groups=mesh['z'=8,'yh'=4,'yl'=2,'tp'=8] {'yh','yl'}, dimensions={0} | all-to-all | bytes 1179648 | tf_op jit(solution)/shard_map/all_to_all | solution.py:365
  30.7 0.0 all-gather.2.cloned.1.call-update
  30.7 0.6 pad_add_fusion.place_ref
  31.4 0.0 copy-start
  31.4 0.0 copy-start.2
  31.4 0.0 copy-start.3
  31.4 0.0 copy-start.4
  31.4 0.0 copy-start.5
  31.4 0.0 copy-start.6
  31.4 0.0 copy-start.9
  31.4 0.0 copy-start.10
  31.4 6.5 %mixer_local.1 = (bf16[8,64,512]{2,1,0:T(8,128)(2,1)S(1)}, f32[2,64,256]{2,1,0:T(8,128)S(1)}) custom-call(s32[3]{0:T(128)} %pad_add_fusion.place_ref, bf16[64,128]{1,0:T(8,128)(2,1)} %reads_ref.3, bf16[64,128]{1,0:T(8,128)(2,1)} %keys_ref.3, bf16[64,128]{1,0:T(8,128)(2,1)} %values_ref.3, bf16[2,64,128]{2,1,0:T(8,128)(2,1)} %fades_ref.1, ...), custom_call_target="tpu_custom_call" | custom-call | flops 1600000000 | tf_op jit(solution)/shard_map/mixer_local/pallas_call | solution.py:369
  37.9 0.0 copy-start.1
  37.9 0.0 copy-start.7
  38.0 16.0 %all_to_all.31.got_ref = bf16[8,64,512]{2,1,0:T(8,128)(2,1)S(1)} all-to-all(bf16[8,64,512]{2,1,0:T(8,128)(2,1)S(1)} %get-tuple-element.9), channel_id=1, replica_groups=mesh['z'=8,'yh'=4,'yl'=2,'tp'=8] {'yh','yl'}, dimensions={0} | all-to-all | bytes 1048576 | tf_op jit(solution)/shard_map/all_to_all | solution.py:365
  54.0 2.0 %combine_near.1 = (bf16[8,64,256]{2,1,0:T(8,128)(2,1)S(1)}, f32[2,64,256]{2,1,0:T(8,128)S(1)}) custom-call(s32[3]{0:T(128)} %pad_add_fusion.place_ref, bf16[8,64,512]{2,1,0:T(8,128)(2,1)S(1)} %all_to_all.31.got_ref), custom_call_target="tpu_custom_call" | custom-call | flops 600000000 | tf_op jit(solution)/shard_map/combine_near/pallas_call | solution.py:381
  56.0 26.3 %all_to_all.32.got_ref = bf16[8,64,256]{2,1,0:T(8,128)(2,1)S(1)} all-to-all(bf16[8,64,256]{2,1,0:T(8,128)(2,1)S(1)} %get-tuple-element.10), channel_id=1, replica_groups=mesh['z'=8,'yh'=4,'yl'=2,'tp'=8] {'z'}, dimensions={0} | all-to-all | bytes 524288 | tf_op jit(solution)/shard_map/all_to_all | solution.py:365
  82.3 0.0 copy-done
  82.3 0.0 copy-done.2
  82.3 0.0 copy-done.3
  82.3 0.0 copy-done.4
  82.3 0.0 copy-done.5
  82.3 0.0 copy-done.6
  82.4 0.0 copy-done.9
  82.4 0.0 copy-done.10
  82.4 2.6 %finish_mixer.1 = bf16[8,8,2048]{2,1,0:T(8,128)(2,1)S(1)} custom-call(s32[3]{0:T(128)} %pad_add_fusion.place_ref, bf16[8,64,256]{2,1,0:T(8,128)(2,1)S(1)} %all_to_all.32.got_ref, f32[2,64,256]{2,1,0:T(8,128)S(1)} %get-tuple-element.11.pre_ref, f32[2,64,256]{2,1,0:T(8,128)S(1)} %get-tuple-element.12.local_ref, bf16[64,128]{1,0:T(8,128)(2,1)S(1)} %copy-done.3, ...), custom_call_target="tpu_custom_call" | custom-call | flops 800000000 | tf_op jit(solution)/shard_map/finish_mixer/pallas_call | solution.py:392
  85.0 15.4 %all_to_all.33.got_ref = bf16[8,8,2048]{2,1,0:T(8,128)(2,1)S(1)} all-to-all(bf16[8,8,2048]{2,1,0:T(8,128)(2,1)S(1)} %finish_mixer.1), channel_id=1, replica_groups=mesh['z'=8,'yh'=4,'yl'=2,'tp'=8] {'tp'}, dimensions={0} | all-to-all | bytes 524288 | tf_op jit(solution)/shard_map/all_to_all | solution.py:365
  100.3 0.0 copy-start.8
  100.3 0.0 copy-done.1
  100.3 0.0 copy-done.7
  100.3 1.1 middle_rows.1.middle_ref
  101.4 13.2 %all_to_all.34 = bf16[16,8,2048]{2,1,0:T(8,128)(2,1)S(1)} all-to-all(bf16[16,8,2048]{2,1,0:T(8,128)(2,1)S(1)} %middle_rows.1.middle_ref), channel_id=1, replica_groups=mesh['z'=8,'yh'=4,'yl'=2,'tp'=8] {'yl','tp'}, dimensions={0} | all-to-all | bytes 1048576 | tf_op jit(solution)/shard_map/all_to_all | solution.py:365
  114.6 0.0 all-gather.2.cloned.1.call-done.weights_ref
  114.6 3.2 %feed_forward.1 = bf16[16,8,2048]{2,1,0:T(8,128)(2,1)S(1)} custom-call(bf16[128,2048]{1,0:T(8,128)(2,1)S(1)} %bitcast.10, bf16[2048,1152]{1,0:T(8,128)(2,1)} %all-gather.2.cloned.1.call-done.weights_ref), custom_call_target="tpu_custom_call" | custom-call | flops 800000000 | tf_op jit(solution)/shard_map/feed_forward/pallas_call | solution.py:414
  117.8 13.5 %all_to_all.35.got_ref = bf16[16,8,2048]{2,1,0:T(8,128)(2,1)S(1)} all-to-all(bf16[16,8,2048]{2,1,0:T(8,128)(2,1)S(1)} %feed_forward.1), channel_id=1, replica_groups=mesh['z'=8,'yh'=4,'yl'=2,'tp'=8] {'yl','tp'}, dimensions={0} | all-to-all | bytes 1048576 | tf_op jit(solution)/shard_map/all_to_all | solution.py:365
  131.3 0.0 copy-done.8
  131.3 0.9 closing_rows.1
Async XLA Ops:
  6.5 108.0 %all-gather.2.cloned.1.call-start = ((), (), s32[]{:S(2)}) async-start(), calls=%async_computation.6 | async-start | bytes 5308416 | tf_op jit(solution)/shard_map/all_gather | solution.py:481
  31.4 50.9 %copy-start = (bf16[128,2048]{1,0:T(8,128)(2,1)S(1)}, bf16[128,2048]{1,0:T(8,128)(2,1)}, u32[]{:S(2)}) copy-start(bf16[128,2048]{1,0:T(8,128)(2,1)} %projector_ref.1) | copy-start | bytes 1572868
  31.4 50.9 %copy-start.2 = (bf16[2,64,128]{2,1,0:T(8,128)(2,1)S(1)}, bf16[2,64,128]{2,1,0:T(8,128)(2,1)}, u32[]{:S(2)}) copy-start(bf16[2,64,128]{2,1,0:T(8,128)(2,1)} %rates_ref.3) | copy-start | bytes 98308
  31.4 50.9 %copy-start.3 = (bf16[64,128]{1,0:T(8,128)(2,1)S(1)}, bf16[64,128]{1,0:T(8,128)(2,1)}, u32[]{:S(2)}) copy-start(bf16[64,128]{1,0:T(8,128)(2,1)} %reads_ref.3) | copy-start | bytes 49156
  31.4 50.9 %copy-start.4 = (bf16[64,128]{1,0:T(8,128)(2,1)S(1)}, bf16[64,128]{1,0:T(8,128)(2,1)}, u32[]{:S(2)}) copy-start(bf16[64,128]{1,0:T(8,128)(2,1)} %keys_ref.3) | copy-start | bytes 49156
  31.4 51.0 %copy-start.5 = (bf16[64,128]{1,0:T(8,128)(2,1)S(1)}, bf16[64,128]{1,0:T(8,128)(2,1)}, u32[]{:S(2)}) copy-start(bf16[64,128]{1,0:T(8,128)(2,1)} %values_ref.3) | copy-start | bytes 49156
  31.4 51.0 %copy-start.6 = (bf16[64,128]{1,0:T(8,128)(2,1)S(1)}, bf16[64,128]{1,0:T(8,128)(2,1)}, u32[]{:S(2)}) copy-start(bf16[64,128]{1,0:T(8,128)(2,1)} %valve_ref.2) | copy-start | bytes 49156
  31.4 50.9 %copy-start.9 = (f32[128]{0:T(128)S(1)}, f32[128]{0:T(128)}, u32[]{:S(2)}) copy-start(f32[128]{0:T(128)} %param.24) | copy-start | bytes 1540
  31.4 50.9 %copy-start.10 = (f32[128]{0:T(128)S(1)}, f32[128]{0:T(128)}, u32[]{:S(2)}) copy-start(f32[128]{0:T(128)} %param.25) | copy-start | bytes 1540
  37.9 62.4 %copy-start.1 = (bf16[64,2048]{1,0:T(8,128)(2,1)S(1)}, bf16[64,2048]{1,0:T(8,128)(2,1)}, u32[]{:S(2)}) copy-start(bf16[64,2048]{1,0:T(8,128)(2,1)} %skip_ref.1) | copy-start | bytes 786436
  37.9 62.4 %copy-start.7 = (f32[2048]{0:T(1024)S(1)}, f32[2048]{0:T(1024)}, u32[]{:S(2)}) copy-start(f32[2048]{0:T(1024)} %param.27) | copy-start | bytes 24580
  100.3 30.9 %copy-start.8 = (f32[2048]{0:T(1024)S(1)}, f32[2048]{0:T(1024)}, u32[]{:S(2)}) copy-start(f32[2048]{0:T(1024)} %param.31) | copy-start | bytes 24580
Sparse Core Ops, SparseCore 0:
  30.8 71.3 all-gather.1

commit v5 on v4

--- a/solution.py
+++ b/solution.py
@@ -190,7 +190,7 @@
     return joined_heads(out), state
 
 
-def mixer_local(place_ref, reads_ref, keys_ref, values_ref, fades_ref, rates_ref, extra_ref, send_ref, out_ref):
+def mixer_local(reads_ref, keys_ref, values_ref, fades_ref, rates_ref, extra_ref, send_ref, out_ref):
     reads, keys = reads_ref[...].astype(F32), keys_ref[...].astype(F32)
     values = values_ref[...].astype(F32)
     unit = keys * lax.rsqrt(head_sums(keys * keys) + KEY_EPS)
@@ -218,8 +218,9 @@
     return moved + jnp.concatenate([piece[:, :WIDE], jnp.zeros((HEAD, WIDE), F32)], axis=1)
 
 
-def combine_near(place_ref, got_ref, send_ref, pre_ref):
-    y, z = place_ref[0], place_ref[1]
+def combine_near(got_ref, send_ref, pre_ref):
+    y = lax.axis_index("yh") * 2 + lax.axis_index("yl")
+    z = lax.axis_index("z")
     start = jnp.concatenate([jnp.zeros((HEAD, WIDE), F32), head_eye()], axis=1)
     total, before = [start, start], [start, start]
     for step in range(8):
@@ -237,7 +238,6 @@
 
 
 def finish_mixer(
-    place_ref,
     got_ref,
     pre_ref,
     local_ref,
@@ -251,7 +251,7 @@
     projector_ref,
     send_ref,
 ):
-    z = place_ref[1]
+    z = lax.axis_index("z")
     state = [jnp.zeros((HEAD, WIDE), F32)] * 2
     for step in range(7):
         for way in range(2):
@@ -283,9 +283,9 @@
     return off * lax.rsqrt(spread + NORM_EPS) * gain
 
 
-def middle_rows(place_ref, got_ref, skip_ref, gain_ref, send_ref):
+def middle_rows(got_ref, skip_ref, gain_ref, send_ref):
     summed = jnp.sum(got_ref[...].astype(F32), axis=0)
-    mine = skip_ref[pl.ds(pl.multiple_of(place_ref[2] * 8, 8), 8), :]
+    mine = skip_ref[pl.ds(pl.multiple_of(lax.axis_index("tp") * 8, 8), 8), :]
     summed = summed + RESIDUAL_SCALE * mine.astype(F32)
     middle = normed_rows(summed, gain_ref[...]).astype(BF16)
     for peer in range(send_ref.shape[0]):
@@ -365,49 +365,49 @@
     return lax.all_to_all(value, axis, 0, 0, tiled=True)
 
 
-def run_mixer_local(place, *args):
+def run_mixer_local(*args):
     return pl.pallas_call(
         mixer_local,
         grid=(1,),
-        in_specs=[SMEM] + [whole(a) for a in args],
+        in_specs=[whole(a) for a in args],
         out_specs=[VMEM] * 2,
         out_shape=[shape((8, HEAD, 4 * WIDE)), shape((2, TOK, 2 * WIDE), F32)],
         cost_estimate=cost(8),
         name="mixer_local",
-    )(place, *args)
-
-
-def run_combine_near(place, got):
+    )(*args)
+
+
+def run_combine_near(got):
     return pl.pallas_call(
         combine_near,
-        in_specs=[SMEM, VMEM],
+        in_specs=[VMEM],
         out_specs=[VMEM] * 2,
         out_shape=[shape((8, HEAD, 2 * WIDE)), shape((2, HEAD, 2 * WIDE), F32)],
         cost_estimate=cost(3),
         name="combine_near",
-    )(place, *near(got))
-
-
-def run_finish_mixer(place, *args):
+    )(*near(got))
+
+
+def run_finish_mixer(*args):
     return pl.pallas_call(
         finish_mixer,
-        in_specs=[SMEM] + [VMEM] * (len(args)),
+        in_specs=[VMEM] * len(args),
         out_specs=VMEM,
         out_shape=shape((8, 8, D)),
         cost_estimate=cost(4),
         name="finish_mixer",
-    )(place, *near(*args))
-
-
-def run_middle_rows(place, got, skip, gain, peers):
+    )(*near(*args))
+
+
+def run_middle_rows(got, skip, gain, peers):
     return pl.pallas_call(
         middle_rows,
-        in_specs=[SMEM] + [VMEM] * 3,
+        in_specs=[VMEM] * 3,
         out_specs=VMEM,
         out_shape=shape((peers, 8, D)),
         cost_estimate=cost(2),
         name="middle_rows",
-    )(place, *near(got, skip, gain))
+    )(*near(got, skip, gain))
 
 
 def run_feed_forward(rows, weights):
@@ -454,9 +454,6 @@
     perceptron_shrink_factors,
     closing_scaling_vector,
 ):
-    place = jnp.stack([lax.axis_index(Y), lax.axis_index("z"), lax.axis_index("tp")]).astype(
-        jnp.int32
-    )
     given = (perceptron_valve_factors, perceptron_widen_factors, perceptron_shrink_factors.T)
     packed = pl.pallas_call(
         pack_weights,
@@ -469,7 +466,6 @@
     )(*given)
     own = exchanged(packed, Y).reshape(PLANE, 3 * PART)
     sends, local = run_mixer_local(
-        place,
         reading_vectors,
         blender_lookup_labels,
         blender_payloads,
@@ -479,10 +475,9 @@
     )
     near_states = exchanged(sends, Y)
     weights = [lax.all_gather(own, "z", axis=0, tiled=True)]
-    totals, before = run_combine_near(place, near_states)
+    totals, before = run_combine_near(near_states)
     far_states = exchanged(totals, "z")
     shares = run_finish_mixer(
-        place,
         far_states,
         before,
         local,
@@ -497,7 +492,7 @@
     )
     shares = exchanged(shares, "tp")
     middle = run_middle_rows(
-        place, shares, skip_stream_entering, blender_scaling_vector.reshape(1, D), PEER_COUNT
+        shares, skip_stream_entering, blender_scaling_vector.reshape(1, D), PEER_COUNT
     )
     rows = exchanged(middle, PEERS).reshape(PEER_COUNT * 8, D)
     down = run_feed_forward(rows, weights[0])

time: 139 us -> 137 us (0.986)
  Pallas kernels: 17.1 us -> 15 us
    pallas_call x4, Pallas kernels: 12.1 us -> 9.98 us  [the longest x1 6.48 us: run_mixer_local(): pl.pallas_call(mixer_local, grid=(1,), in_specs=[whole(a) for a in args],...]
  transfers between devices with their start and end apart: 1 -> 1, of which waited for: 0 -> 0; matrix products, arithmetic and copies ran while one was open for 0% -> 0% of each run, Pallas kernels for 9% -> 7%
where the time goes in v5:
time: 137 us; the launch traced here: 136 us
  blocking collectives  108 us (79%)
  Pallas kernels  15 us (11%)
  between operations  13.6 us (10%)
    all_to_all x6, blocking collectives, exchanged(): return lax.all_to_all(value, axis, 0, 0, tiled=True)  108 us
    pallas_call x1, Pallas kernels, run_mixer_local(): pl.pallas_call(mixer_local, grid=(1,), in_specs=[whole(a) for a in args],...  6.48 us
    pallas_call x1, Pallas kernels, run_feed_forward(): pl.pallas_call(feed_forward, in_specs=[VMEM, pl.BlockSpec(memory_space=pl...  3.22 us
  transfers between devices with their start and end apart: 1, of which 0 were waited for; matrix products, arithmetic and copies ran while one was open for 0% of the time, Pallas kernels for 7%

profile of v5, /device:TPU:1, one launch (start us, length us, event | category | flops | bytes accessed | tf_op | source)
XLA Modules:
  0.0 136.2 jit_solution(10671156602694921634)
XLA Ops:
  6.5 0.0 all-gather.2.cloned.1.call-start
  6.5 0.9 pack_weights.1
  7.4 23.3 %all_to_all.30 = bf16[8,32,1152]{2,1,0:T(8,128)(2,1)} all-to-all(bf16[8,32,1152]{2,1,0:T(8,128)(2,1)S(1)} %pack_weights.1), channel_id=1, replica_groups=mesh['z'=8,'yh'=4,'yl'=2,'tp'=8] {'yh','yl'}, dimensions={0} | all-to-all | bytes 1179648 | tf_op jit(solution)/shard_map/all_to_all | solution.py:365
  30.7 0.0 all-gather.2.cloned.1.call-update
  30.7 0.0 copy-start
  30.7 0.0 copy-start.2
  30.7 0.0 copy-start.3
  30.8 0.0 copy-start.4
  30.8 0.0 copy-start.5
  30.8 0.0 copy-start.6
  30.8 0.0 copy-start.9
  30.8 0.0 copy-start.10
  30.8 6.5 %mixer_local.1 = (bf16[8,64,512]{2,1,0:T(8,128)(2,1)S(1)}, f32[2,64,256]{2,1,0:T(8,128)S(1)}) custom-call(bf16[64,128]{1,0:T(8,128)(2,1)} %reads_ref.3, bf16[64,128]{1,0:T(8,128)(2,1)} %keys_ref.3, bf16[64,128]{1,0:T(8,128)(2,1)} %values_ref.3, bf16[2,64,128]{2,1,0:T(8,128)(2,1)} %fades_ref.1, bf16[2,64,128]{2,1,0:T(8,128)(2,1)} %rates_ref.3, ...), custom_call_target="tpu_custom_call" | custom-call | flops 1600000000 | tf_op jit(solution)/shard_map/mixer_local/pallas_call | solution.py:369
  37.3 0.0 copy-start.1
  37.3 0.0 copy-start.7
  37.3 16.0 %all_to_all.31.got_ref = bf16[8,64,512]{2,1,0:T(8,128)(2,1)S(1)} all-to-all(bf16[8,64,512]{2,1,0:T(8,128)(2,1)S(1)} %get-tuple-element.9), channel_id=1, replica_groups=mesh['z'=8,'yh'=4,'yl'=2,'tp'=8] {'yh','yl'}, dimensions={0} | all-to-all | bytes 1048576 | tf_op jit(solution)/shard_map/all_to_all | solution.py:365
  53.4 1.3 combine_near.1
  54.7 26.3 %all_to_all.32.got_ref = bf16[8,64,256]{2,1,0:T(8,128)(2,1)S(1)} all-to-all(bf16[8,64,256]{2,1,0:T(8,128)(2,1)S(1)} %get-tuple-element.10), channel_id=1, replica_groups=mesh['z'=8,'yh'=4,'yl'=2,'tp'=8] {'z'}, dimensions={0} | all-to-all | bytes 524288 | tf_op jit(solution)/shard_map/all_to_all | solution.py:365
  81.0 0.0 copy-done
  81.0 0.0 copy-done.2
  81.0 0.0 copy-done.3
  81.0 0.0 copy-done.4
  81.0 0.0 copy-done.5
  81.0 0.0 copy-done.6
  81.0 0.0 copy-done.9
  81.0 0.0 copy-done.10
  81.1 1.9 %finish_mixer.1 = bf16[8,8,2048]{2,1,0:T(8,128)(2,1)S(1)} custom-call(bf16[8,64,256]{2,1,0:T(8,128)(2,1)S(1)} %all_to_all.32.got_ref, f32[2,64,256]{2,1,0:T(8,128)S(1)} %get-tuple-element.11.pre_ref, f32[2,64,256]{2,1,0:T(8,128)S(1)} %get-tuple-element.12.local_ref, bf16[64,128]{1,0:T(8,128)(2,1)S(1)} %copy-done.3, bf16[64,128]{1,0:T(8,128)(2,1)S(1)} %copy-done.4, ...), custom_call_target="tpu_custom_call" | custom-call | flops 800000000 | tf_op jit(solution)/shard_map/finish_mixer/pallas_call | solution.py:392
  83.0 15.4 %all_to_all.33.got_ref = bf16[8,8,2048]{2,1,0:T(8,128)(2,1)S(1)} all-to-all(bf16[8,8,2048]{2,1,0:T(8,128)(2,1)S(1)} %finish_mixer.1), channel_id=1, replica_groups=mesh['z'=8,'yh'=4,'yl'=2,'tp'=8] {'tp'}, dimensions={0} | all-to-all | bytes 524288 | tf_op jit(solution)/shard_map/all_to_all | solution.py:365
  98.4 0.0 copy-start.8
  98.4 0.0 copy-done.1
  98.4 0.0 copy-done.7
  98.4 0.3 middle_rows.1.middle_ref
  98.6 13.2 %all_to_all.34 = bf16[16,8,2048]{2,1,0:T(8,128)(2,1)S(1)} all-to-all(bf16[16,8,2048]{2,1,0:T(8,128)(2,1)S(1)} %middle_rows.1.middle_ref), channel_id=1, replica_groups=mesh['z'=8,'yh'=4,'yl'=2,'tp'=8] {'yl','tp'}, dimensions={0} | all-to-all | bytes 1048576 | tf_op jit(solution)/shard_map/all_to_all | solution.py:365
  111.8 0.0 all-gather.2.cloned.1.call-done.weights_ref
  111.8 3.2 %feed_forward.1 = bf16[16,8,2048]{2,1,0:T(8,128)(2,1)S(1)} custom-call(bf16[128,2048]{1,0:T(8,128)(2,1)S(1)} %bitcast.7, bf16[2048,1152]{1,0:T(8,128)(2,1)} %all-gather.2.cloned.1.call-done.weights_ref), custom_call_target="tpu_custom_call" | custom-call | flops 800000000 | tf_op jit(solution)/shard_map/feed_forward/pallas_call | solution.py:414
  115.1 13.4 %all_to_all.35.got_ref = bf16[16,8,2048]{2,1,0:T(8,128)(2,1)S(1)} all-to-all(bf16[16,8,2048]{2,1,0:T(8,128)(2,1)S(1)} %feed_forward.1), channel_id=1, replica_groups=mesh['z'=8,'yh'=4,'yl'=2,'tp'=8] {'yl','tp'}, dimensions={0} | all-to-all | bytes 1048576 | tf_op jit(solution)/shard_map/all_to_all | solution.py:365
  128.5 0.0 copy-done.8
  128.5 0.9 closing_rows.1
Async XLA Ops:
  6.5 105.3 %all-gather.2.cloned.1.call-start = ((), (), s32[]{:S(2)}) async-start(), calls=%async_computation.6 | async-start | bytes 5308416 | tf_op jit(solution)/shard_map/all_gather | solution.py:477
  30.7 50.3 %copy-start = (bf16[128,2048]{1,0:T(8,128)(2,1)S(1)}, bf16[128,2048]{1,0:T(8,128)(2,1)}, u32[]{:S(2)}) copy-start(bf16[128,2048]{1,0:T(8,128)(2,1)} %projector_ref.1) | copy-start | bytes 1572868
  30.7 50.3 %copy-start.2 = (bf16[2,64,128]{2,1,0:T(8,128)(2,1)S(1)}, bf16[2,64,128]{2,1,0:T(8,128)(2,1)}, u32[]{:S(2)}) copy-start(bf16[2,64,128]{2,1,0:T(8,128)(2,1)} %rates_ref.3) | copy-start | bytes 98308
  30.7 50.3 %copy-start.3 = (bf16[64,128]{1,0:T(8,128)(2,1)S(1)}, bf16[64,128]{1,0:T(8,128)(2,1)}, u32[]{:S(2)}) copy-start(bf16[64,128]{1,0:T(8,128)(2,1)} %reads_ref.3) | copy-start | bytes 49156
  30.8 50.2 %copy-start.4 = (bf16[64,128]{1,0:T(8,128)(2,1)S(1)}, bf16[64,128]{1,0:T(8,128)(2,1)}, u32[]{:S(2)}) copy-start(bf16[64,128]{1,0:T(8,128)(2,1)} %keys_ref.3) | copy-start | bytes 49156
  30.8 50.2 %copy-start.5 = (bf16[64,128]{1,0:T(8,128)(2,1)S(1)}, bf16[64,128]{1,0:T(8,128)(2,1)}, u32[]{:S(2)}) copy-start(bf16[64,128]{1,0:T(8,128)(2,1)} %values_ref.3) | copy-start | bytes 49156
  30.8 50.2 %copy-start.6 = (bf16[64,128]{1,0:T(8,128)(2,1)S(1)}, bf16[64,128]{1,0:T(8,128)(2,1)}, u32[]{:S(2)}) copy-start(bf16[64,128]{1,0:T(8,128)(2,1)} %valve_ref.2) | copy-start | bytes 49156
  30.8 50.2 %copy-start.9 = (f32[128]{0:T(128)S(1)}, f32[128]{0:T(128)}, u32[]{:S(2)}) copy-start(f32[128]{0:T(128)} %param.24) | copy-start | bytes 1540
  30.8 50.2 %copy-start.10 = (f32[128]{0:T(128)S(1)}, f32[128]{0:T(128)}, u32[]{:S(2)}) copy-start(f32[128]{0:T(128)} %param.25) | copy-start | bytes 1540
  37.3 61.1 %copy-start.1 = (bf16[64,2048]{1,0:T(8,128)(2,1)S(1)}, bf16[64,2048]{1,0:T(8,128)(2,1)}, u32[]{:S(2)}) copy-start(bf16[64,2048]{1,0:T(8,128)(2,1)} %skip_ref.1) | copy-start | bytes 786436
  37.3 61.1 %copy-start.7 = (f32[2048]{0:T(1024)S(1)}, f32[2048]{0:T(1024)}, u32[]{:S(2)}) copy-start(f32[2048]{0:T(1024)} %param.27) | copy-start | bytes 24580
  98.4 30.1 %copy-start.8 = (f32[2048]{0:T(1024)S(1)}, f32[2048]{0:T(1024)}, u32[]{:S(2)}) copy-start(f32[2048]{0:T(1024)} %param.31) | copy-start | bytes 24580
Sparse Core Ops, SparseCore 0:
  30.8 71.3 all-gather.1

commit v6 on v5

--- a/solution.py
+++ b/solution.py
@@ -250,7 +250,11 @@
     gain_ref,
     projector_ref,
     send_ref,
+    held_ref,
+    arrived,
 ):
+    copy = pltpu.make_async_copy(projector_ref, held_ref, arrived)
+    copy.start()
     z = lax.axis_index("z")
     state = [jnp.zeros((HEAD, WIDE), F32)] * 2
     for step in range(7):
@@ -273,7 +277,8 @@
     bonus = head_sums(reads_ref[...].astype(F32) * both * reward_ref[...])
     bonus = bonus * values_ref[...].astype(F32)
     mixed = ((normed + bonus) * valve_ref[...].astype(F32)).astype(BF16)
-    share = jnp.dot(mixed, projector_ref[...], preferred_element_type=F32)
+    copy.wait()
+    share = jnp.dot(mixed, held_ref[...], preferred_element_type=F32)
     send_ref[...] = share.astype(BF16).reshape(send_ref.shape)
 
 
@@ -373,6 +378,7 @@
         out_specs=[VMEM] * 2,
         out_shape=[shape((8, HEAD, 4 * WIDE)), shape((2, TOK, 2 * WIDE), F32)],
         cost_estimate=cost(8),
+        compiler_params=pltpu.CompilerParams(vmem_limit_bytes=66_200_000),
         name="mixer_local",
     )(*args)
 
@@ -389,14 +395,16 @@
 
 
 def run_finish_mixer(*args):
+    *args, projector = args
     return pl.pallas_call(
         finish_mixer,
-        in_specs=[VMEM] * len(args),
+        in_specs=[VMEM] * len(args) + [pl.BlockSpec(memory_space=pl.ANY)],
         out_specs=VMEM,
         out_shape=shape((8, 8, D)),
+        scratch_shapes=[pltpu.VMEM((WIDE, D), BF16), pltpu.SemaphoreType.DMA(())],
         cost_estimate=cost(4),
         name="finish_mixer",
-    )(*near(*args))
+    )(*near(*args), projector)
 
 
 def run_middle_rows(got, skip, gain, peers):

time: 137 us -> 138 us (level)
  transfers between devices with their start and end apart: 1 -> 1, of which waited for: 0 -> 0; matrix products, arithmetic and copies ran while one was open for 0% -> 0% of each run, Pallas kernels for 7% -> 8%
where the time goes in v6:
time: 138 us; the launch traced here: 137 us
  blocking collectives  108 us (78%)
  Pallas kernels  15.8 us (11%)
  between operations  13.5 us (10%)
    all_to_all x6, blocking collectives, exchanged(): return lax.all_to_all(value, axis, 0, 0, tiled=True)  108 us
    pallas_call x1, Pallas kernels, run_mixer_local(): pl.pallas_call(mixer_local, grid=(1,), in_specs=[whole(a) for a in args],...  6.49 us
    pallas_call x1, Pallas kernels, run_feed_forward(): pl.pallas_call(feed_forward, in_specs=[VMEM, pl.BlockSpec(memory_space=pl...  3.22 us
  transfers between devices with their start and end apart: 1, of which 0 were waited for; matrix products, arithmetic and copies ran while one was open for 0% of the time, Pallas kernels for 8%

profile of v6, /device:TPU:1, one launch (start us, length us, event | category | flops | bytes accessed | tf_op | source)
XLA Modules:
  0.0 137.1 jit_solution(6820517370429776072)
XLA Ops:
  6.5 0.0 all-gather.2.cloned.1.call-start
  6.5 0.9 pack_weights.1
  7.4 23.3 %all_to_all.30 = bf16[8,32,1152]{2,1,0:T(8,128)(2,1)} all-to-all(bf16[8,32,1152]{2,1,0:T(8,128)(2,1)S(1)} %pack_weights.1), channel_id=1, replica_groups=mesh['z'=8,'yh'=4,'yl'=2,'tp'=8] {'yh','yl'}, dimensions={0} | all-to-all | bytes 1179648 | tf_op jit(solution)/shard_map/all_to_all | solution.py:370
  30.7 0.0 all-gather.2.cloned.1.call-update
  30.7 0.0 copy-start.1
  30.7 0.0 copy-start.2
  30.7 0.0 copy-start.3
  30.8 0.0 copy-start.4
  30.8 0.0 copy-start.5
  30.8 0.0 copy-start.8
  30.8 0.0 copy-start.9
  30.8 6.5 %mixer_local.1 = (bf16[8,64,512]{2,1,0:T(8,128)(2,1)S(1)}, f32[2,64,256]{2,1,0:T(8,128)S(1)}) custom-call(bf16[64,128]{1,0:T(8,128)(2,1)} %reads_ref.3, bf16[64,128]{1,0:T(8,128)(2,1)} %keys_ref.3, bf16[64,128]{1,0:T(8,128)(2,1)} %values_ref.3, bf16[2,64,128]{2,1,0:T(8,128)(2,1)} %fades_ref.1, bf16[2,64,128]{2,1,0:T(8,128)(2,1)} %rates_ref.3, ...), custom_call_target="tpu_custom_call" | custom-call | flops 1600000000 | tf_op jit(solution)/shard_map/mixer_local/pallas_call | solution.py:374
  37.3 0.0 copy-start
  37.3 0.0 copy-start.6
  37.3 16.0 %all_to_all.31.got_ref = bf16[8,64,512]{2,1,0:T(8,128)(2,1)S(1)} all-to-all(bf16[8,64,512]{2,1,0:T(8,128)(2,1)S(1)} %get-tuple-element.9), channel_id=1, replica_groups=mesh['z'=8,'yh'=4,'yl'=2,'tp'=8] {'yh','yl'}, dimensions={0} | all-to-all | bytes 1048576 | tf_op jit(solution)/shard_map/all_to_all | solution.py:370
  53.4 1.3 combine_near.1
  54.7 26.3 %all_to_all.32.got_ref = bf16[8,64,256]{2,1,0:T(8,128)(2,1)S(1)} all-to-all(bf16[8,64,256]{2,1,0:T(8,128)(2,1)S(1)} %get-tuple-element.10), channel_id=1, replica_groups=mesh['z'=8,'yh'=4,'yl'=2,'tp'=8] {'z'}, dimensions={0} | all-to-all | bytes 524288 | tf_op jit(solution)/shard_map/all_to_all | solution.py:370
  81.0 0.0 copy-done.1
  81.0 0.0 copy-done.2
  81.0 0.0 copy-done.3
  81.0 0.0 copy-done.4
  81.0 0.0 copy-done.5
  81.0 0.0 copy-done.8
  81.0 0.0 copy-done.9
  81.0 2.8 %finish_mixer.1 = bf16[8,8,2048]{2,1,0:T(8,128)(2,1)S(1)} custom-call(bf16[8,64,256]{2,1,0:T(8,128)(2,1)S(1)} %all_to_all.32.got_ref, f32[2,64,256]{2,1,0:T(8,128)S(1)} %get-tuple-element.11.pre_ref, f32[2,64,256]{2,1,0:T(8,128)S(1)} %get-tuple-element.12.local_ref, bf16[64,128]{1,0:T(8,128)(2,1)S(1)} %copy-done.2, bf16[64,128]{1,0:T(8,128)(2,1)S(1)} %copy-done.3, ...), custom_call_target="tpu_custom_call" | custom-call | flops 800000000 | tf_op jit(solution)/shard_map/finish_mixer/pallas_call | solution.py:399
  83.8 15.4 %all_to_all.33.got_ref = bf16[8,8,2048]{2,1,0:T(8,128)(2,1)S(1)} all-to-all(bf16[8,8,2048]{2,1,0:T(8,128)(2,1)S(1)} %finish_mixer.1), channel_id=1, replica_groups=mesh['z'=8,'yh'=4,'yl'=2,'tp'=8] {'tp'}, dimensions={0} | all-to-all | bytes 524288 | tf_op jit(solution)/shard_map/all_to_all | solution.py:370
  99.2 0.0 copy-start.7
  99.2 0.0 copy-done
  99.2 0.0 copy-done.6
  99.2 0.3 middle_rows.1.middle_ref
  99.5 13.2 %all_to_all.34 = bf16[16,8,2048]{2,1,0:T(8,128)(2,1)S(1)} all-to-all(bf16[16,8,2048]{2,1,0:T(8,128)(2,1)S(1)} %middle_rows.1.middle_ref), channel_id=1, replica_groups=mesh['z'=8,'yh'=4,'yl'=2,'tp'=8] {'yl','tp'}, dimensions={0} | all-to-all | bytes 1048576 | tf_op jit(solution)/shard_map/all_to_all | solution.py:370
  112.6 0.0 all-gather.2.cloned.1.call-done.weights_ref
  112.6 3.2 %feed_forward.1 = bf16[16,8,2048]{2,1,0:T(8,128)(2,1)S(1)} custom-call(bf16[128,2048]{1,0:T(8,128)(2,1)S(1)} %bitcast.7, bf16[2048,1152]{1,0:T(8,128)(2,1)} %all-gather.2.cloned.1.call-done.weights_ref), custom_call_target="tpu_custom_call" | custom-call | flops 800000000 | tf_op jit(solution)/shard_map/feed_forward/pallas_call | solution.py:422
  115.9 13.5 %all_to_all.35.got_ref = bf16[16,8,2048]{2,1,0:T(8,128)(2,1)S(1)} all-to-all(bf16[16,8,2048]{2,1,0:T(8,128)(2,1)S(1)} %feed_forward.1), channel_id=1, replica_groups=mesh['z'=8,'yh'=4,'yl'=2,'tp'=8] {'yl','tp'}, dimensions={0} | all-to-all | bytes 1048576 | tf_op jit(solution)/shard_map/all_to_all | solution.py:370
  129.3 0.0 copy-done.7
  129.3 0.9 closing_rows.1
Async XLA Ops:
  6.5 106.1 %all-gather.2.cloned.1.call-start = ((), (), s32[]{:S(2)}) async-start(), calls=%async_computation.6 | async-start | bytes 5308416 | tf_op jit(solution)/shard_map/all_gather | solution.py:485
  30.7 50.3 %copy-start.1 = (bf16[2,64,128]{2,1,0:T(8,128)(2,1)S(1)}, bf16[2,64,128]{2,1,0:T(8,128)(2,1)}, u32[]{:S(2)}) copy-start(bf16[2,64,128]{2,1,0:T(8,128)(2,1)} %rates_ref.3) | copy-start | bytes 98308
  30.7 50.3 %copy-start.2 = (bf16[64,128]{1,0:T(8,128)(2,1)S(1)}, bf16[64,128]{1,0:T(8,128)(2,1)}, u32[]{:S(2)}) copy-start(bf16[64,128]{1,0:T(8,128)(2,1)} %reads_ref.3) | copy-start | bytes 49156
  30.7 50.3 %copy-start.3 = (bf16[64,128]{1,0:T(8,128)(2,1)S(1)}, bf16[64,128]{1,0:T(8,128)(2,1)}, u32[]{:S(2)}) copy-start(bf16[64,128]{1,0:T(8,128)(2,1)} %keys_ref.3) | copy-start | bytes 49156
  30.8 50.2 %copy-start.4 = (bf16[64,128]{1,0:T(8,128)(2,1)S(1)}, bf16[64,128]{1,0:T(8,128)(2,1)}, u32[]{:S(2)}) copy-start(bf16[64,128]{1,0:T(8,128)(2,1)} %values_ref.3) | copy-start | bytes 49156
  30.8 50.2 %copy-start.5 = (bf16[64,128]{1,0:T(8,128)(2,1)S(1)}, bf16[64,128]{1,0:T(8,128)(2,1)}, u32[]{:S(2)}) copy-start(bf16[64,128]{1,0:T(8,128)(2,1)} %valve_ref.2) | copy-start | bytes 49156
  30.8 50.2 %copy-start.8 = (f32[128]{0:T(128)S(1)}, f32[128]{0:T(128)}, u32[]{:S(2)}) copy-start(f32[128]{0:T(128)} %param.24) | copy-start | bytes 1540
  30.8 50.2 %copy-start.9 = (f32[128]{0:T(128)S(1)}, f32[128]{0:T(128)}, u32[]{:S(2)}) copy-start(f32[128]{0:T(128)} %param.25) | copy-start | bytes 1540
  37.3 61.9 %copy-start = (bf16[64,2048]{1,0:T(8,128)(2,1)S(1)}, bf16[64,2048]{1,0:T(8,128)(2,1)}, u32[]{:S(2)}) copy-start(bf16[64,2048]{1,0:T(8,128)(2,1)} %skip_ref.1) | copy-start | bytes 786436
  37.3 61.9 %copy-start.6 = (f32[2048]{0:T(1024)S(1)}, f32[2048]{0:T(1024)}, u32[]{:S(2)}) copy-start(f32[2048]{0:T(1024)} %param.27) | copy-start | bytes 24580
  99.2 30.1 %copy-start.7 = (f32[2048]{0:T(1024)S(1)}, f32[2048]{0:T(1024)}, u32[]{:S(2)}) copy-start(f32[2048]{0:T(1024)} %param.31) | copy-start | bytes 24580
Sparse Core Ops, SparseCore 0:
  30.8 71.3 all-gather.1
